TPU v7x, 512 devices: a whole 4x8x8 slice. The times are simulated.
512 devices in a mesh: sp: 64 (over z, y), tp: 8 (over x, core).
Axes of the slice: x: 4, y: 8, z: 8, core: 2. Of those that a mesh axis runs over, the one named last changes fastest.
Arguments:
- hidden_in: bfloat16 [32768, 2048], P('sp'), may hold values from -64 to 64
- pre_gain: float32 [2048], replicated, may hold values from 0.1 to 1.9
- query_proj: bfloat16 [2048, 2048], P(None, 'tp'), may hold values from -2 to 2
- key_proj: bfloat16 [2048, 2048], P('sp', 'tp'), may hold values from -2 to 2
- value_proj: bfloat16 [2048, 2048], P('sp', 'tp'), may hold values from -0.125 to 0.125
- out_proj: bfloat16 [2048, 2048], P('tp'), may hold values from -0.125 to 0.125
- post_gain: float32 [2048], replicated, may hold values from 0.1 to 1.9
Outputs:
- layer_out: bfloat16 [32768, 2048], P(('sp', 'tp'))
- log_weight: float32 [32, 32768], P('tp', 'sp')
All inputs are finite; a program needn't handle non-finite values.
Results may differ from a plain program's by a relative error of at most 0.018.
The roundings to bfloat16 on the way count: a program that leaves them out, or rounds other values in their place, can miss the bound.
Values may be sent and summed in bfloat16 or wider, within the bound.
A program may use at most 64 MiB of HBM per device.

v0:
```python
import jax
import jax.numpy as jnp
from jax import lax
from jax.sharding import PartitionSpec as P

HEAD_DIM = 64
SPAN = 128


EPS = 1e-06
ROPE_BASE = 10000.0
DILATIONS = (1, 4, 16)


def side_by_side(arrays, axis, dim, along):
    widths = [a.shape[along] for a in arrays]
    both = jnp.concatenate(arrays, axis=along)
    whole = lax.all_gather(both, axis, axis=dim, tiled=True)
    return tuple(jnp.split(whole, [sum(widths[:k]) for k in range(1, len(widths))], axis=along))


def passed_along(value, axis, steps):
    count = lax.axis_size(axis)
    first, last = (max(0, -steps), min(count, count - steps))
    return lax.ppermute(value, axis, [(source, source + steps) for source in range(first, last)])


def split_up(x, dim, peers):
    dims = x.shape
    parts = x.reshape(*dims[:dim], peers, dims[dim] // peers, *dims[dim + 1 :])
    return jnp.moveaxis(parts, dim, 0)


def sum_at_owner(x, axis, dim):
    parts = split_up(x, dim, lax.axis_size(axis))
    arrived = lax.all_to_all(parts, axis, split_axis=0, concat_axis=0, tiled=True)
    return arrived.astype(jnp.float32).sum(axis=0)


def rotate(vectors, positions):
    half_dim = vectors.shape[-1] // 2
    frequency = ROPE_BASE ** (-(jnp.arange(half_dim, dtype=jnp.float32) * 2.0 / vectors.shape[-1]))
    angles = positions[:, None] * frequency[None, :]
    cos_part = jnp.cos(angles)[:, None, :]
    sin_part = jnp.sin(angles)[:, None, :]
    front_half = vectors[..., :half_dim]
    back_half = vectors[..., half_dim:]
    return jnp.concatenate(
        [
            front_half * cos_part - back_half * sin_part,
            back_half * cos_part + front_half * sin_part,
        ],
        axis=-1,
    )


def rms_scale(matrix, gain):
    return matrix * lax.rsqrt(jnp.mean(matrix * matrix, axis=-1, keepdims=True) + EPS) * gain


def window_group(queries, buffer, dilation, offset):
    local_rows, head_count, head_depth = queries.shape
    reach_rows = dilation * SPAN
    start_row = buffer.shape[1] - local_rows - reach_rows
    key_rows = buffer[0, start_row:]
    value_rows = buffer[1, start_row:]
    res_len = local_rows // dilation
    block_len = min(SPAN, res_len)
    blocks = res_len // block_len
    query_blocks = queries.reshape(blocks, block_len, dilation, head_count, head_depth)
    key_res = key_rows.reshape(-1, dilation, head_count, head_depth)
    value_res = value_rows.reshape(-1, dilation, head_count, head_depth)
    width_keys = block_len + SPAN
    key_sets = jnp.stack(
        [
            key_res[block_idx * block_len : block_idx * block_len + width_keys]
            for block_idx in range(blocks)
        ]
    )
    value_sets = jnp.stack(
        [
            value_res[block_idx * block_len : block_idx * block_len + width_keys]
            for block_idx in range(blocks)
        ]
    )
    scores = jnp.einsum(
        "bqrhe,bkrhe->brhqk", query_blocks, key_sets, preferred_element_type=jnp.float32
    ) * head_depth ** (-0.5)
    query_idx = jnp.arange(block_len, dtype=jnp.int32)[:, None]
    key_idx = jnp.arange(width_keys, dtype=jnp.int32)[None, :]
    distance = query_idx + SPAN - key_idx
    in_band = (distance >= 0) & (distance <= SPAN)
    key_pos = (
        (
            jnp.arange(blocks, dtype=jnp.int32)[:, None, None, None, None] * block_len
            + jnp.arange(width_keys, dtype=jnp.int32)[None, None, None, None, :]
        )
        * dilation
        + jnp.arange(dilation, dtype=jnp.int32)[None, :, None, None, None]
        + (offset - reach_rows)
    )
    valid = in_band[None, None, None] & (key_pos >= 0)
    scores = jnp.where(valid, scores, -jnp.inf)
    row_max = jnp.max(scores, axis=-1, keepdims=True)
    exp_scores = jnp.exp(scores - row_max)
    denominator = jnp.sum(exp_scores, axis=-1, keepdims=True)
    levels = (row_max + jnp.log(denominator))[..., 0]
    shares = (exp_scores / denominator).astype(jnp.bfloat16)
    outcome = jnp.einsum(
        "brhqk,bkrhe->bqrhe", shares, value_sets, preferred_element_type=jnp.float32
    )
    outcome = outcome.reshape(local_rows, head_count, head_depth)
    levels = levels.transpose(2, 0, 3, 1).reshape(head_count, local_rows)
    return (outcome, levels)


def blend(group_outs, group_levels):
    levels = jnp.stack(group_levels)
    row_max = jnp.max(levels, axis=0)
    log_weight = row_max + jnp.log(jnp.sum(jnp.exp(levels - row_max[None]), axis=0))
    shares = jnp.exp(levels - log_weight[None])
    blended = jnp.sum(shares.transpose(0, 2, 1)[..., None] * jnp.stack(group_outs), axis=0)
    return (blended, log_weight)


def body(hidden_in, pre_gain, query_proj, key_proj, value_proj, out_proj, post_gain):
    local_rows = hidden_in.shape[0]
    local_width = query_proj.shape[1]
    head_count = local_width // HEAD_DIM
    normed = rms_scale(hidden_in.astype(jnp.float32), pre_gain).astype(jnp.bfloat16)
    offset = lax.axis_index("sp") * local_rows
    positions = (offset + jnp.arange(local_rows, dtype=jnp.int32)).astype(jnp.float32)
    queries = rotate(
        jnp.dot(normed, query_proj, preferred_element_type=jnp.float32).reshape(
            local_rows, head_count, HEAD_DIM
        ),
        positions,
    ).astype(jnp.bfloat16)
    pieces = side_by_side((key_proj, value_proj), "sp", 0, 1)
    key_sum = jnp.dot(normed, pieces[0], preferred_element_type=jnp.float32)
    value_sum = jnp.dot(normed, pieces[1], preferred_element_type=jnp.float32)
    key_rows = (
        rotate(key_sum.reshape(local_rows, head_count, HEAD_DIM), positions)
        .astype(jnp.bfloat16)
        .reshape(local_rows, local_width)
    )
    key_value = jnp.stack([key_rows, value_sum.astype(jnp.bfloat16)])
    behind = -(-(16 * SPAN) // local_rows)
    pieces = [key_value]
    current = key_value
    for section in range(behind):
        current = passed_along(current, "sp", 1)
        pieces.insert(0, current)
    buffer = jnp.concatenate(pieces, axis=1)
    buffer = buffer.reshape(2, buffer.shape[1], head_count, HEAD_DIM)
    group_outs = []
    group_levels = []
    for dilation in DILATIONS:
        outcome, levels = window_group(queries, buffer, dilation, offset)
        group_outs.append(outcome)
        group_levels.append(levels)
    blended, log_weight = blend(group_outs, group_levels)
    attended = blended.astype(jnp.bfloat16).reshape(local_rows, local_width)
    summed = sum_at_owner(
        jnp.dot(attended, out_proj, preferred_element_type=jnp.float32).astype(jnp.bfloat16),
        "tp",
        0,
    )
    layer_out = rms_scale(summed, post_gain).astype(jnp.bfloat16)
    return (layer_out, log_weight)


def solution(mesh):
    placed = (P("sp", None), P(), P(None, "tp"), P("sp", "tp"), P("sp", "tp"), P("tp", None), P())
    return jax.shard_map(
        body,
        mesh=mesh,
        in_specs=placed,
        out_specs=(P(("sp", "tp"), None), P("tp", "sp")),
        check_vma=False,
    )
```

profile of v0, /device:TPU:1, one launch (start us, length us, event | category | flops | bytes accessed | tf_op | source)
XLA Modules:
  0.0 259.2 jit_solution(949253217690158348)
XLA Ops:
  7.2 1.5 pad_maximum_fusion.2
  8.8 2.1 fusion
  11.3 2.9 %fusion.73 = f32[512,256]{0,1:T(8,128)} fusion(bf16[2048,256]{1,0:T(8,128)(2,1)} %param.9, bf16[512,2048]{1,0:T(8,128)(2,1)S(1)} %copy-done.3, f32[2048]{0:T(1024)S(1)} %copy-done.37, f32[512]{0:T(512)S(1)} %add_rsqrt_fusion), kind=kOutput, calls=%fused_computation.139 | convolution fusion | flops 541065216 | bytes 3680256 | tf_op jit(solution)/shard_map/dot_general | solution.py:134
  14.2 82.1 %all-gather.2.cloned.1.call-done = bf16[2048,512]{1,0:T(8,128)(2,1)} async-done(((bf16[32,512]{1,0:T(8,128)(2,1)}), bf16[2048,512]{1,0:T(8,128)(2,1)}) %all-gather.2.cloned.1.call-update) | async-done | bytes 2097168 | tf_op jit(solution)/shard_map/all_gather | solution.py:18
  96.3 2.2 fusion.19
  98.9 2.6 %fusion.17 = bf16[1,512,256]{2,1,0:T(8,128)(2,1)S(1)} fusion(bf16[2048,512]{1,0:T(8,128)(2,1)} %all-gather.2.cloned.1.call-done, bf16[512,2048]{1,0:T(8,128)(2,1)} %param.7, f32[2048]{0:T(1024)S(1)} %copy-done.37, f32[512]{0:T(512)S(1)} %add_rsqrt_fusion), kind=kOutput, calls=%fused_computation.32 | convolution fusion | flops 541196288 | bytes 3418112 | tf_op jit(solution)/shard_map/dot_general | solution.py:141
  101.6 2.7 %collective-permute-start = (bf16[2,512,256]{2,1,0:T(8,128)(2,1)S(1)}, bf16[2,512,256]{2,1,0:T(8,128)(2,1)S(1)}, u32[]{:S(2)}, u32[]{:S(2)}) collective-permute-start(bf16[2,512,256]{2,1,0:T(8,128)(2,1)S(1)} %pad_maximum_fusion), channel_id=1, source_target_pairs={{0,8},{8,16},{16,24},{24,32},{32,40},{40,48},{48,56},{56,64},{64,7... | collective-permute-start | bytes 1572872 | tf_op jit(solution)/shard_map/ppermute | solution.py:25
  104.4 6.2 %collective-permute-done = bf16[2,512,256]{2,1,0:T(8,128)(2,1)S(1)} collective-permute-done((bf16[2,512,256]{2,1,0:T(8,128)(2,1)S(1)}, bf16[2,512,256]{2,1,0:T(8,128)(2,1)S(1)}, u32[]{:S(2)}, u32[]{:S(2)}) %collective-permute-start) | collective-permute-done | bytes 524320 | tf_op jit(solution)/shard_map/ppermute | solution.py:25
  110.6 4.1 %collective-permute-start.1 = (bf16[2,512,256]{2,1,0:T(8,128)(2,1)S(1)}, bf16[2,512,256]{2,1,0:T(8,128)(2,1)S(1)}, u32[]{:S(2)}, u32[]{:S(2)}) collective-permute-start(bf16[2,512,256]{2,1,0:T(8,128)(2,1)S(1)} %collective-permute-done), channel_id=1, source_target_pairs={{0,8},{8,16},{16,24},{24,32},{32,40},{40,48},{48,56},{56,64},{64,7... | collective-permute-start | bytes 1572872 | tf_op jit(solution)/shard_map/ppermute | solution.py:25
  114.9 6.7 %collective-permute-done.1 = bf16[2,512,256]{2,1,0:T(8,128)(2,1)S(1)} collective-permute-done((bf16[2,512,256]{2,1,0:T(8,128)(2,1)S(1)}, bf16[2,512,256]{2,1,0:T(8,128)(2,1)S(1)}, u32[]{:S(2)}, u32[]{:S(2)}) %collective-permute-start.1) | collective-permute-done | bytes 524320 | tf_op jit(solution)/shard_map/ppermute | solution.py:25
  121.6 4.6 %collective-permute-start.2 = (bf16[2,512,256]{2,1,0:T(8,128)(2,1)S(1)}, bf16[2,512,256]{2,1,0:T(8,128)(2,1)}, u32[]{:S(2)}, u32[]{:S(2)}) collective-permute-start(bf16[2,512,256]{2,1,0:T(8,128)(2,1)S(1)} %collective-permute-done.1), channel_id=1, source_target_pairs={{0,8},{8,16},{16,24},{24,32},{32,40},{40,48},{48,56},{56,64},{64,7... | collective-permute-start | bytes 1572872 | tf_op jit(solution)/shard_map/ppermute | solution.py:25
  127.1 6.3 %collective-permute-done.2 = bf16[2,512,256]{2,1,0:T(8,128)(2,1)} collective-permute-done((bf16[2,512,256]{2,1,0:T(8,128)(2,1)S(1)}, bf16[2,512,256]{2,1,0:T(8,128)(2,1)}, u32[]{:S(2)}, u32[]{:S(2)}) %collective-permute-start.2) | collective-permute-done | bytes 524320 | tf_op jit(solution)/shard_map/ppermute | solution.py:25
  133.5 4.7 %collective-permute-start.3 = (bf16[2,512,256]{2,1,0:T(8,128)(2,1)}, bf16[2,512,256]{2,1,0:T(8,128)(2,1)}, u32[]{:S(2)}, u32[]{:S(2)}) collective-permute-start(bf16[2,512,256]{2,1,0:T(8,128)(2,1)} %collective-permute-done.2), channel_id=1, source_target_pairs={{0,8},{8,16},{16,24},{24,32},{32,40},{40,48},{48,56},{56,64},{64,7... | collective-permute-start | bytes 1572872 | tf_op jit(solution)/shard_map/ppermute | solution.py:25
  144.0 3.0 %collective-permute-done.3 = bf16[2,512,256]{2,1,0:T(8,128)(2,1)} collective-permute-done((bf16[2,512,256]{2,1,0:T(8,128)(2,1)}, bf16[2,512,256]{2,1,0:T(8,128)(2,1)}, u32[]{:S(2)}, u32[]{:S(2)}) %collective-permute-start.3) | collective-permute-done | bytes 524320 | tf_op jit(solution)/shard_map/ppermute | solution.py:25
  146.9 1.9 constant_dynamic-update-slice_fusion.4
  148.8 1.9 constant_dynamic-update-slice_fusion.3
  153.2 4.4 %copy.55 = bf16[2,2560,256]{1,2,0:T(8,128)(2,1)} copy(bf16[2,2560,256]{2,1,0:T(8,128)(2,1)} %constant_dynamic-update-slice_fusion) | data formatting | bytes 5242880 | tf_op jit(solution)/shard_map/concatenate | solution.py:154
  157.6 3.1 %fusion.76 = (bf16[1,2560,256]{2,1,0:T(8,128)(2,1)S(1)}, bf16[1,2560,256]{2,1,0:T(8,128)(2,1)}) fusion(bf16[2,2560,256]{2,1,0:T(8,128)(2,1)} %constant_dynamic-update-slice_fusion), kind=kLoop, calls=%fused_computation.141 | loop fusion | bytes 5242880 | tf_op jit(solution)/shard_map/slice | solution.py:65
  161.8 1.2 fusion.75
  162.9 2.1 reshape.508
  165.0 5.0 %fusion.10 = (f32[16,4,32]{2,1,0:T(4,128)S(1)}, f32[16,4,32,160]{3,2,1,0:T(8,128)S(1)}) fusion(pred[16,32,160]{2,1,0:T(8,128)(4,1)S(1)} %broadcast_and_fusion, bf16[160,16,4,64]{3,2,1,0:T(4,128)(2,1)} %reshape.508, bf16[32,16,4,32]{3,0,2,1:T(8,128)(2,1)} %copy.66, bf16[32,16,4,32]{3,0,2,1:T(8,128)(2,1)} %copy.65), kind=kOutput, calls=%fused_computation.24 | convolution fusion | flops 43448320 | bytes 2973696 | tf_op jit(solution)/shard_map/bqrhe,bkrhe->brhqk/dot_general | solution.py:86
  173.0 2.4 copy.60
  175.4 2.0 fusion.9
  179.0 1.6 fusion.11
  184.2 2.4 copy.73
  186.6 3.9 %convolution_bitcast_fusion = f32[1,128,4,4,64]{1,4,3,2,0:T(8,128)} fusion(bf16[256,4,4,64]{3,1,0,2:T(4,128)(2,1)} %bitcast.115, f32[4,4,128,256]{3,2,1,0:T(8,128)} %copy-done.6, f32[4,4,128]{2,1,0:T(4,128)} %copy-done.32, f32[4,4,128]{2,1,0:T(4,128)} %copy-done.31, pred[4,128,256]{2,1,0:T(8,128)(4,1)} %get-tuple-element.21), kind=kOutput, calls=%fused_computation.29 | convolution fusion | flops 69730304 | bytes 3293184 | tf_op jit(solution)/shard_map/brhqk,bkrhe->bqrhe/dot_general | solution.py:109
  192.7 2.4 copy.75
  195.1 2.1 copy.78
  197.2 4.9 %reshape.511 = bf16[160,16,4,64]{3,2,1,0:T(4,128)(2,1)} reshape(bf16[1,2560,256]{2,1,0:T(8,128)(2,1)} %get-tuple-element.13) | data formatting | bytes 2621440 | tf_op jit(solution)/shard_map/reshape.69
  202.2 3.6 %fusion.14 = f32[1,32,16,4,64]{4,1,3,2,0:T(8,128)S(1)} fusion(bf16[160,16,4,64]{3,2,1,0:T(4,128)(2,1)} %reshape.511, f32[16,4,32,160]{3,2,1,0:T(8,128)S(1)} %get-tuple-element.25, f32[16,4,32]{2,1,0:T(4,128)S(1)} %copy-done.18, f32[16,4,32]{2,1,0:T(4,128)S(1)} %copy-done.16, pred[16,32,160]{2,1,0:T(8,128)(4,1)S(1)} %broadcast_and_fusion), kind=kOutput, calls=%fused_computation.28 | convolution fusion | flops 43581440 | bytes 3244032 | tf_op jit(solution)/shard_map/brhqk,bkrhe->bqrhe/dot_general | solution.py:109
  206.9 3.6 %fusion.7 = bf16[512,4,64]{0,2,1:T(8,128)(2,1)S(1)} fusion(f32[1,512,4,64]{1,0,3,2:T(1,128)S(1)} %copy.79, f32[1,512,4,64]{1,0,3,2:T(1,128)S(1)} %copy-done.2, f32[1,512,4,64]{1,0,3,2:T(1,128)} %bitcast.112, f32[3,512,4]{1,0,2:T(4,128)S(1)} %copy.71), kind=kLoop, calls=%fused_computation.12 | loop fusion | flops 1441792 | bytes 1859584 | tf_op jit(solution)/shard_map/reduce_sum | solution.py:122
  211.2 39.6 %all_to_all.5 = bf16[8,64,2048]{2,1,0:T(8,128)(2,1)S(1)} all-to-all(bf16[8,64,2048]{2,1,0:T(8,128)(2,1)S(1)} %bitcast.103), channel_id=1, replica_groups=mesh['sp'=64,'tp'=8] {'tp'}, dimensions={0} | all-to-all | bytes 4194304 | tf_op jit(solution)/shard_map/all_to_all | solution.py:36
  (135 shorter events, 24.7 us)
Async XLA Ops:
  7.2 203.3 %copy-start = (bf16[256,2048]{1,0:T(8,128)(2,1)S(1)}, bf16[256,2048]{1,0:T(8,128)(2,1)}, u32[]{:S(2)}) copy-start(bf16[256,2048]{1,0:T(8,128)(2,1)} %param.12) | copy-start | bytes 3145732
  7.2 4.1 %copy-start.3 = (bf16[512,2048]{1,0:T(8,128)(2,1)S(1)}, bf16[512,2048]{1,0:T(8,128)(2,1)}, u32[]{:S(2)}) copy-start(bf16[512,2048]{1,0:T(8,128)(2,1)} %param.7) | copy-start | bytes 6291460
  7.2 4.1 %copy-start.37 = (f32[2048]{0:T(1024)S(1)}, f32[2048]{0:T(1024)}, u32[]{:S(2)}) copy-start(f32[2048]{0:T(1024)} %param.8) | copy-start | bytes 24580
  7.2 89.1 %all-gather.2.cloned.1.call-start = ((), (), s32[]{:S(2)}) async-start(), calls=%async_computation.1 | async-start | bytes 2129920 | tf_op jit(solution)/shard_map/all_gather | solution.py:18
  96.3 2.2 copy-start.14
  101.6 9.1 %collective-permute-start = (bf16[2,512,256]{2,1,0:T(8,128)(2,1)S(1)}, bf16[2,512,256]{2,1,0:T(8,128)(2,1)S(1)}, u32[]{:S(2)}, u32[]{:S(2)}) collective-permute-start(bf16[2,512,256]{2,1,0:T(8,128)(2,1)S(1)} %pad_maximum_fusion), channel_id=1, source_target_pairs={{0,8},{8,16},{16,24},{24,32},{32,40},{40,48},{48,56},{56,64},{64,7... | collective-permute-start | bytes 1572872 | tf_op jit(solution)/shard_map/ppermute | solution.py:25
  110.6 27.6 %copy-start.10 = (bf16[2,512,256]{2,1,0:T(8,128)(2,1)}, bf16[2,512,256]{2,1,0:T(8,128)(2,1)S(1)}, u32[]{:S(2)}) copy-start(bf16[2,512,256]{2,1,0:T(8,128)(2,1)S(1)} %collective-permute-done) | copy-start | bytes 1572868
  110.6 11.0 %collective-permute-start.1 = (bf16[2,512,256]{2,1,0:T(8,128)(2,1)S(1)}, bf16[2,512,256]{2,1,0:T(8,128)(2,1)S(1)}, u32[]{:S(2)}, u32[]{:S(2)}) collective-permute-start(bf16[2,512,256]{2,1,0:T(8,128)(2,1)S(1)} %collective-permute-done), channel_id=1, source_target_pairs={{0,8},{8,16},{16,24},{24,32},{32,40},{40,48},{48,56},{56,64},{64,7... | collective-permute-start | bytes 1572872 | tf_op jit(solution)/shard_map/ppermute | solution.py:25
  121.6 16.6 %copy-start.12 = (bf16[2,512,256]{2,1,0:T(8,128)(2,1)}, bf16[2,512,256]{2,1,0:T(8,128)(2,1)S(1)}, u32[]{:S(2)}) copy-start(bf16[2,512,256]{2,1,0:T(8,128)(2,1)S(1)} %collective-permute-done.1) | copy-start | bytes 1572868
  121.6 11.8 %collective-permute-start.2 = (bf16[2,512,256]{2,1,0:T(8,128)(2,1)S(1)}, bf16[2,512,256]{2,1,0:T(8,128)(2,1)}, u32[]{:S(2)}, u32[]{:S(2)}) collective-permute-start(bf16[2,512,256]{2,1,0:T(8,128)(2,1)S(1)} %collective-permute-done.1), channel_id=1, source_target_pairs={{0,8},{8,16},{16,24},{24,32},{32,40},{40,48},{48,56},{56,64},{64,7... | collective-permute-start | bytes 1572872 | tf_op jit(solution)/shard_map/ppermute | solution.py:25
  127.1 51.1 %copy-start.7 = (pred[4,128,256]{2,1,0:T(8,128)(4,1)}, pred[4,128,256]{2,1,0:T(8,128)(4,1)S(1)}, u32[]{:S(2)}) copy-start(pred[4,128,256]{2,1,0:T(8,128)(4,1)S(1)} %get-tuple-element.20) | copy-start | bytes 393220
  133.5 13.5 %collective-permute-start.3 = (bf16[2,512,256]{2,1,0:T(8,128)(2,1)}, bf16[2,512,256]{2,1,0:T(8,128)(2,1)}, u32[]{:S(2)}, u32[]{:S(2)}) collective-permute-start(bf16[2,512,256]{2,1,0:T(8,128)(2,1)} %collective-permute-done.2), channel_id=1, source_target_pairs={{0,8},{8,16},{16,24},{24,32},{32,40},{40,48},{48,56},{56,64},{64,7... | collective-permute-start | bytes 1572872 | tf_op jit(solution)/shard_map/ppermute | solution.py:25
  141.7 9.0 %copy-start.13 = (bf16[2,512,256]{2,1,0:T(8,128)(2,1)S(1)}, bf16[2,512,256]{2,1,0:T(8,128)(2,1)}, u32[]{:S(2)}) copy-start(bf16[2,512,256]{2,1,0:T(8,128)(2,1)} %copy-done.12) | copy-start | bytes 1572868
  142.6 8.9 %copy-start.11 = (bf16[2,512,256]{2,1,0:T(8,128)(2,1)S(1)}, bf16[2,512,256]{2,1,0:T(8,128)(2,1)}, u32[]{:S(2)}) copy-start(bf16[2,512,256]{2,1,0:T(8,128)(2,1)} %copy-done.10) | copy-start | bytes 1572868
  157.6 3.1 %copy-start.1 = (bf16[2,2560,256]{1,2,0:T(8,128)(2,1)S(1)}, bf16[2,2560,256]{1,2,0:T(8,128)(2,1)}, u32[]{:S(2)}) copy-start(bf16[2,2560,256]{1,2,0:T(8,128)(2,1)} %copy.55) | copy-start | bytes 7864324
  175.4 2.1 copy-start.23
  175.4 2.1 copy-start.24
  175.4 2.1 copy-start.25
  175.4 2.1 copy-start.26
  175.4 2.1 copy-start.27
  175.4 2.1 copy-start.28
  177.5 3.1 %copy-start.31 = (f32[4,4,128]{2,1,0:T(4,128)}, f32[4,4,128]{2,1,0:T(4,128)S(1)}, u32[]{:S(2)}) copy-start(f32[4,4,128]{2,1,0:T(4,128)S(1)} %get-tuple-element.26) | copy-start | bytes 24580
  178.2 2.4 copy-start.4
  186.5 4.0 %copy-start.5 = (f32[4,4,128,256]{3,2,1,0:T(8,128)S(1)}, f32[4,4,128,256]{3,2,1,0:T(8,128)}, u32[]{:S(2)}) copy-start(f32[4,4,128,256]{3,2,1,0:T(8,128)} %copy-done.4) | copy-start | bytes 6291460
  186.5 4.0 %copy-start.8 = (pred[4,128,256]{2,1,0:T(8,128)(4,1)S(1)}, pred[4,128,256]{2,1,0:T(8,128)(4,1)}, u32[]{:S(2)}) copy-start(pred[4,128,256]{2,1,0:T(8,128)(4,1)} %copy-done.7) | copy-start | bytes 393220
  186.5 4.0 %copy-start.19 = (bf16[1,256,1,4,64]{1,4,3,0,2:T(8,128)(2,1)S(1)}, bf16[1,256,1,4,64]{1,4,3,0,2:T(8,128)(2,1)}, u32[]{:S(2)}) copy-start(bf16[1,256,1,4,64]{1,4,3,0,2:T(8,128)(2,1)} %get-tuple-element.2) | copy-start | bytes 393220
  186.5 4.0 %copy-start.20 = (bf16[1,256,1,4,64]{1,4,3,0,2:T(8,128)(2,1)S(1)}, bf16[1,256,1,4,64]{1,4,3,0,2:T(8,128)(2,1)}, u32[]{:S(2)}) copy-start(bf16[1,256,1,4,64]{1,4,3,0,2:T(8,128)(2,1)} %get-tuple-element.3) | copy-start | bytes 393220
  186.5 4.0 %copy-start.21 = (bf16[1,256,1,4,64]{1,4,3,0,2:T(8,128)(2,1)S(1)}, bf16[1,256,1,4,64]{1,4,3,0,2:T(8,128)(2,1)}, u32[]{:S(2)}) copy-start(bf16[1,256,1,4,64]{1,4,3,0,2:T(8,128)(2,1)} %get-tuple-element.4) | copy-start | bytes 393220
  186.6 4.0 %copy-start.22 = (bf16[1,256,1,4,64]{1,4,3,0,2:T(8,128)(2,1)S(1)}, bf16[1,256,1,4,64]{1,4,3,0,2:T(8,128)(2,1)}, u32[]{:S(2)}) copy-start(bf16[1,256,1,4,64]{1,4,3,0,2:T(8,128)(2,1)} %get-tuple-element.5) | copy-start | bytes 393220
  192.7 9.5 %copy-start.34 = (f32[4,512]{1,0:T(4,128)}, f32[4,512]{1,0:T(4,128)S(1)}, u32[]{:S(2)}) copy-start(f32[4,512]{1,0:T(4,128)S(1)} %log_add_fusion) | copy-start | bytes 24580
  197.2 4.9 %copy-start.16 = (f32[16,4,32]{2,1,0:T(4,128)S(1)}, f32[16,4,32]{2,1,0:T(4,128)}, u32[]{:S(2)}) copy-start(f32[16,4,32]{2,1,0:T(4,128)} %copy-done.15) | copy-start | bytes 24580
  197.2 4.9 %copy-start.18 = (f32[16,4,32]{2,1,0:T(4,128)S(1)}, f32[16,4,32]{2,1,0:T(4,128)}, u32[]{:S(2)}) copy-start(f32[16,4,32]{2,1,0:T(4,128)} %copy-done.17) | copy-start | bytes 24580
  (11 other events, 14.9 us)
Sparse Core Ops, SparseCore 0:
  11.6 84.6 all-gather.1
where the time goes:
time: 263 us; the launch traced here: 259 us
  waiting for transfers between devices  104 us (40%)
  local copies, waits for them, and re-layouts  45.7 us (17%)
  blocking collectives  39.6 us (15%)
  matrix products  24.4 us (9%)
  starting transfers between devices  16.2 us (6%)
  between operations  14.7 us (6%)
  other arithmetic  14.2 us (5%)
    all_gather x1, waiting for transfers between devices, side_by_side(): whole = lax.all_gather(both, axis, axis=dim, tiled=True)  82.1 us
    all_to_all x1, blocking collectives, sum_at_owner(): lax.all_to_all(parts, axis, split_axis=0, concat_axis=0, tiled=True)  39.6 us
    ppermute x4, waiting for transfers between devices, passed_along(): lax.ppermute(value, axis, [(source, source + steps) for source in range(f...  22.3 us
    ppermute x4, starting transfers between devices, passed_along(): lax.ppermute(value, axis, [(source, source + steps) for source in range(f...  16.2 us
    dot_general x3, matrix products, window_group(): jnp.einsum('brhqk,bkrhe->bqrhe', shares, value_sets, preferred_element_ty...  8.3 us
    unnamed x80, local copies, waits for them, and re-layouts  7.71 us
    dot_general x3, matrix products, window_group(): jnp.einsum('bqrhe,bkrhe->brhqk', query_blocks, key_sets, preferred_elemen...  7.62 us
    another operation x4, local copies, waits for them, and re-layouts  7.53 us
  transfers between devices with their start and end apart: 5, of which 5 were waited for; matrix products, arithmetic and copies ran while one was open for 5% of the time, Pallas kernels for 0%

commit v1 on v0

v1 whole, which is shorter than its diff:
```python
import functools
import math

import jax
import jax.numpy as jnp
import numpy as np
from jax import lax
from jax.experimental import pallas as pl
from jax.experimental.pallas import tpu as pltpu
from jax.sharding import PartitionSpec as P

HEAD_DIM = 64
SPAN = 128
EPS = 1e-06
ROPE_BASE = 10000.0
NY = 8
NZ = 8
NSP = NY * NZ
NTP = 8
NX = 4
ROWS = 512
D = 2048
WIDTH = 256
OUT_ROWS = 64
SLOTS = 5
NEG = -1e30
SCALE2 = math.log2(math.e) / 8.0
LN2 = math.log(2.0)
F32 = jnp.float32
BF16 = jnp.bfloat16
MESH = pl.DeviceIdType.MESH

NT = (((1,), (1,)), ((), ()))
NN = (((1,), (0,)), ((), ()))

R_WY = 0
R_WZ = R_WY + 2 * (NY - 1)
R_X = R_WZ + 2 * 2 * 2 * 4
R_H = R_X + 16
R_A = R_H + 2 * SLOTS
R_END = R_A + 2 * (NTP - 1)
N_SEND = 110


def dot(a, b, dims=NN):
    return lax.dot_general(a, b, dims, preferred_element_type=F32)


def token_of(row):
    return (row // 128) + ((row // 8) % 4) * 4 + (row % 8) * 16 + ((row // 32) % 4) * 128


def kernel(
    hid, gain, freq, wq, wk, wv, wo, post,
    out, lw_out,
    hid_v, np_v, wq_v, w_v, wo_v, kv, q_s, st_o, st_m, st_l, att_p, att_n, att_all, lw_s,
    cos_s, sin_s, bias_c, bias_n, perm, sum_s, lsem, ssem, rsem,
):
    sp = lax.axis_index("sp")
    tp = lax.axis_index("tp")
    z, y = sp // NY, sp % NY
    x, core = tp // 2, tp % 2
    sends = []

    def start(src, dst, ridx, dev):
        copy = pltpu.make_async_remote_copy(
            src_ref=src, dst_ref=dst, send_sem=ssem.at[len(sends)], recv_sem=rsem.at[ridx],
            device_id=dev, device_id_type=MESH,
        )
        copy.start()
        sends.append(copy)

    def arrived(dst, ridx):
        pltpu.make_async_remote_copy(
            src_ref=dst, dst_ref=dst, send_sem=ssem.at[0], recv_sem=rsem.at[ridx],
            device_id=((sp + 1) % NSP, tp), device_id_type=MESH,
        ).wait_recv()

    y_peer = [(z * NY + (y + d) % NY, tp) for d in range(NY)]
    z_up = (((z + 1) % NZ) * NY + y, tp)
    z_down = (((z + NZ - 1) % NZ) * NY + y, tp)
    ahead = ((sp + 1) % NSP, tp)
    behind = ((sp + NSP - 1) % NSP, tp)
    t_peer = [(sp, (tp + d) % NTP) for d in range(NTP)]
    x_right = (sp, (tp + 2) % NTP)
    x_left = (sp, (tp + NTP - 2) % NTP)
    sibling = (sp, x * 2 + (1 - core))

    wrow = pl.ds(pl.multiple_of(sp * 32, 32), 32)
    local = [
        pltpu.make_async_copy(wk.at[:, 0:128], w_v.at[0, wrow, 0:128], lsem.at[0]),
        pltpu.make_async_copy(wv.at[:, 0:128], w_v.at[0, wrow, 128:256], lsem.at[1]),
        pltpu.make_async_copy(wk.at[:, 128:256], w_v.at[1, wrow, 0:128], lsem.at[2]),
        pltpu.make_async_copy(wv.at[:, 128:256], w_v.at[1, wrow, 128:256], lsem.at[3]),
        pltpu.make_async_copy(wo, wo_v.at[tp], lsem.at[4]),
        pltpu.make_async_copy(hid, hid_v, lsem.at[5]),
        pltpu.make_async_copy(wq, wq_v, lsem.at[6]),
    ]
    for copy in local:
        copy.start()

    barrier = pltpu.get_barrier_semaphore()
    partners = y_peer[1:] + t_peer[1:] + [z_up, z_down, ahead, behind]
    for dev in partners:
        pl.semaphore_signal(barrier, inc=1, device_id=dev, device_id_type=MESH)
    pl.semaphore_wait(barrier, len(partners))

    def weights_y_send(p):
        local[2 * p].wait()
        local[2 * p + 1].wait()
        for d in range(1, NY):
            start(w_v.at[p, wrow], w_v.at[p, wrow], R_WY + p * (NY - 1) + d - 1, y_peer[d])

    def weights_y_wait(p):
        for d in range(1, NY):
            row = (z * NY + (y + NY - d) % NY) * 32
            arrived(w_v.at[p, pl.ds(pl.multiple_of(row, 32), 32)], R_WY + p * (NY - 1) + d - 1)

    def z_rows(zz, half):
        return pl.ds(pl.multiple_of(zz * 256 + half * 128, 128), 128)

    def z_sem(p, half, direction, hop):
        return R_WZ + ((p * 2 + half) * 2 + direction) * 4 + hop

    def z_hops(half, direction):
        return 4 if half == direction else 3

    def weights_z_send(p):
        for half in range(2):
            part = w_v.at[p, z_rows(z, half)]
            start(part, part, z_sem(p, half, 0, 0), z_up)
            start(part, part, z_sem(p, half, 1, 0), z_down)

    def weights_z_step(p, hop):
        for half in range(2):
            for direction in range(2):
                hops = z_hops(half, direction)
                if hop < hops:
                    zz = (z + NZ - 1 - hop) % NZ if direction == 0 else (z + 1 + hop) % NZ
                    part = w_v.at[p, z_rows(zz, half)]
                    arrived(part, z_sem(p, half, direction, hop))
                    if hop + 1 < hops:
                        start(part, part, z_sem(p, half, direction, hop + 1), z_up if direction == 0 else z_down)

    def wo_part(delta, part):
        group = wo_v.at[(tp + delta) % NTP]
        return group if part is None else group.at[pl.ds(part * 128, 128)]

    def wo_send():
        local[4].wait()
        start(wo_part(0, 0), wo_part(0, 0), R_X + 0, x_right)
        start(wo_part(0, 1), wo_part(0, 1), R_X + 1, x_left)
        start(wo_part(0, 1), wo_part(0, 1), R_X + 2, x_right)
        start(wo_part(0, 0), wo_part(0, 0), R_X + 3, x_left)
        start(wo_part(0, None), wo_part(0, None), R_X + 6, sibling)

    def wo_step(k):
        if k == 0:
            arrived(wo_part(6, 0), R_X + 0)
            start(wo_part(6, 0), wo_part(6, 0), R_X + 4, x_right)
            start(wo_part(6, 0), wo_part(6, 0), R_X + 7, sibling)
            arrived(wo_part(2, 1), R_X + 1)
            start(wo_part(2, 1), wo_part(2, 1), R_X + 5, x_left)
            start(wo_part(2, 1), wo_part(2, 1), R_X + 8, sibling)
        elif k == 1:
            arrived(wo_part(6, 1), R_X + 2)
            start(wo_part(6, 1), wo_part(6, 1), R_X + 9, sibling)
            arrived(wo_part(2, 0), R_X + 3)
            start(wo_part(2, 0), wo_part(2, 0), R_X + 10, sibling)
        else:
            arrived(wo_part(4, 0), R_X + 4)
            start(wo_part(4, 0), wo_part(4, 0), R_X + 11, sibling)
            arrived(wo_part(4, 1), R_X + 5)
            start(wo_part(4, 1), wo_part(4, 1), R_X + 12, sibling)

    def wo_sibling_wait():
        other = x * 2 + (1 - core)

        def part_of(delta, part):
            group = wo_v.at[(other + delta) % NTP]
            return group if part is None else group.at[pl.ds(part * 128, 128)]

        arrived(part_of(0, None), R_X + 6)
        arrived(part_of(6, 0), R_X + 7)
        arrived(part_of(2, 1), R_X + 8)
        arrived(part_of(6, 1), R_X + 9)
        arrived(part_of(2, 0), R_X + 10)
        arrived(part_of(4, 0), R_X + 11)
        arrived(part_of(4, 1), R_X + 12)

    def halo_send(p):
        start(kv.at[0, p], kv.at[1, p], R_H + p * SLOTS + 1, ahead)

    def halo_step(p, k):
        arrived(kv.at[k, p], R_H + p * SLOTS + k)
        if k < SLOTS - 1:
            start(kv.at[k, p], kv.at[k + 1, p], R_H + p * SLOTS + k + 1, ahead)

    lane = lax.broadcasted_iota(jnp.int32, (1, 128), 1)
    first_head = lane < 64
    first_half = (lane % 64) < 32

    def norm():
        local[5].wait()

        def step(i, _):
            rows = pl.ds(pl.multiple_of(i * 32, 32), 32)
            h = hid_v[rows, :].astype(F32)
            scale = lax.rsqrt(jnp.mean(h * h, axis=-1, keepdims=True) + EPS)
            hid_v[rows, :] = (h * scale * gain[...]).astype(BF16)
            return 0

        lax.fori_loop(0, ROWS // 32, step, 0)

    def permutation():
        token = token_of(lax.broadcasted_iota(jnp.int32, (ROWS, ROWS), 0))
        col = lax.broadcasted_iota(jnp.int32, (ROWS, ROWS), 1)
        perm[0] = (token == col).astype(F32).astype(BF16)
        row = lax.broadcasted_iota(jnp.int32, (ROWS, ROWS), 0)
        token_c = token_of(lax.broadcasted_iota(jnp.int32, (ROWS, ROWS), 1))
        perm[1] = (token_c == row).astype(F32).astype(BF16)

    def permute():
        def step(i, _):
            rows = pl.ds(pl.multiple_of(i * 128, 128), 128)
            for c in range(4):
                np_v[rows, c * 512 : (c + 1) * 512] = dot(perm[0, rows, :], hid_v[:, c * 512 : (c + 1) * 512]).astype(BF16)
            return 0

        lax.fori_loop(0, 4, step, 0)

    def tables():
        token = token_of(lax.broadcasted_iota(jnp.int32, (ROWS, 128), 0))
        angle = (sp * ROWS + token).astype(F32) * freq[...]
        cos_s[...] = jnp.cos(angle)
        sine = jnp.sin(angle)
        sin_s[...] = jnp.where(first_half, -sine, sine)

    def biases():
        row = lax.broadcasted_iota(jnp.int32, (128, 128), 0)
        col = lax.broadcasted_iota(jnp.int32, (128, 128), 1)

        def class_token(r):
            return (r // 32) * 128 + (r % 8) * 16 + ((r // 8) % 4) * 4

        for k in range(SLOTS):
            delta = class_token(row) - class_token(col) + ROWS * k
            near = (delta >= 0) & (delta <= 4 * SPAN)
            far = (delta >= 0) & (delta <= 16 * SPAN) & ((row // 8) % 4 == (col // 8) % 4)
            bias = jnp.where(near & far, 1.0, jnp.where(near | far, 0.0, NEG))
            bias_c[:, k * 128 : (k + 1) * 128] = jnp.where(sp >= k, bias, NEG)

        def near_token(r):
            return (r // 32) + (r % 8) * 16 + ((r // 8) % 4) * 4

        delta = near_token(row) - near_token(col)
        own = jnp.where((delta >= 0) & (delta <= SPAN), 0.0, NEG)
        delta = delta + 128
        prev = jnp.where((delta >= 0) & (delta <= SPAN), 0.0, NEG)
        bias_n[0, :, 0:128] = jnp.where(sp >= 1, prev, NEG)
        bias_n[1, :, 0:128] = prev
        bias_n[0, :, 128:256] = own
        bias_n[1, :, 128:256] = own

    def rotate(u, rows):
        swapped = jnp.where(first_half, pltpu.roll(u, 96, 1), pltpu.roll(u, 32, 1))
        return (u * cos_s[rows, :] + swapped * sin_s[rows, :]).astype(BF16)

    def queries():
        local[6].wait()

        def step(r, _):
            rows = pl.ds(pl.multiple_of(r * 128, 128), 128)
            q = dot(np_v[rows, :], wq_v[...])
            for p in range(2):
                turned = rotate(q[:, p * 128 : (p + 1) * 128], rows)
                zero = jnp.zeros_like(turned)
                q_s[p, r, 0:128, :] = jnp.where(first_head, turned, zero)
                q_s[p, r, 128:256, :] = jnp.where(first_head, zero, turned)
            return 0

        lax.fori_loop(0, 4, step, 0)

    def keys_values(p):
        def step(r, _):
            rows = pl.ds(pl.multiple_of(r * 128, 128), 128)
            both = dot(np_v[rows, :], w_v[p])
            kv[0, p, 0, rows, :] = rotate(both[:, 0:128], rows)
            kv[0, p, 1, rows, :] = both[:, 128:256].astype(BF16)
            return 0

        lax.fori_loop(0, 4, step, 0)

    def near(p, first, last):
        def step(b, _):
            slot = (3 - b) // 3
            before = (b + 3) % 4

            def part(r, base):
                return pl.ds(pl.multiple_of(base + r * 128, 32), 32)

            q = jnp.concatenate(
                [q_s[p, r, pl.ds(pl.multiple_of(h * 128 + b * 32, 32), 32), :] for h in range(2) for r in range(4)], axis=0
            )
            k, v = (
                jnp.concatenate(
                    [kv[slot, p, w, part(r, before * 32), :] for r in range(4)]
                    + [kv[0, p, w, part(r, b * 32), :] for r in range(4)],
                    axis=0,
                )
                for w in range(2)
            )
            bias = bias_n[jnp.minimum(b, 1)]
            s = dot(q, k, NT) * SCALE2 + jnp.concatenate([bias, bias], axis=0)
            m = jnp.max(s, axis=-1, keepdims=True)
            e = jnp.exp2(s - m)
            total = jnp.sum(e, axis=-1, keepdims=True)
            o = dot(e.astype(BF16), v)
            m = jnp.broadcast_to(m, o.shape)
            total = jnp.broadcast_to(total, o.shape)
            for h in range(2):
                for r in range(4):
                    at = pl.ds(pl.multiple_of(h * 128 + b * 32, 32), 32)
                    piece = slice(h * 128 + r * 32, h * 128 + r * 32 + 32)
                    st_o[p, r, at, :] = o[piece]
                    st_m[p, r, at, :] = m[piece]
                    st_l[p, r, at, :] = total[piece]
            return 0

        lax.fori_loop(first, last, step, 0)

    def far(p, slots):
        def step(r, _):
            rows = pl.ds(pl.multiple_of(r * 128, 128), 128)
            k, v = (
                jnp.concatenate([kv[s, p, w, rows, :] for s in slots], axis=0) if len(slots) > 1 else kv[slots[0], p, w, rows, :]
                for w in range(2)
            )
            bias = bias_c[:, slots[0] * 128 : (slots[-1] + 1) * 128]
            s = dot(q_s[p, r], k, NT) * SCALE2 + jnp.concatenate([bias, bias], axis=0)
            m_old = st_m[p, r]
            m = jnp.maximum(m_old, jnp.broadcast_to(jnp.max(s, axis=-1, keepdims=True), m_old.shape))
            wide = m if len(slots) == 1 else jnp.concatenate([m] * len(slots), axis=1)
            e = jnp.exp2(s - wide)
            decay = jnp.exp2(m_old - m)
            st_l[p, r] = st_l[p, r] * decay + jnp.broadcast_to(jnp.sum(e, axis=-1, keepdims=True), m.shape)
            st_o[p, r] = st_o[p, r] * decay + dot(e.astype(BF16), v)
            st_m[p, r] = m
            return 0

        lax.fori_loop(0, 4, step, 0)

    def finish(p):
        for r in range(4):
            rows = slice(r * 128, (r + 1) * 128)
            o = st_o[p, r] / st_l[p, r]
            att_p[rows, :] = jnp.where(first_head, o[0:128], o[128:256]).astype(BF16)
            level = st_m[p, r] * LN2 + jnp.log(st_l[p, r])
            both = jnp.where(lane == 2 * p, level[0:128], level[128:256])
            if p == 0:
                lw_s[rows, :] = both
            else:
                lw_s[rows, :] = jnp.where(lane < 2, lw_s[rows, :], both)
        att_n[p] = dot(perm[1], att_p[...]).astype(BF16)
        att_all[p, tp] = att_n[p, pl.ds(pl.multiple_of(tp * OUT_ROWS, OUT_ROWS), OUT_ROWS), :]
        for d in range(1, NTP):
            rows = pl.ds(pl.multiple_of(((tp + d) % NTP) * OUT_ROWS, OUT_ROWS), OUT_ROWS)
            start(att_n.at[p, rows], att_all.at[p, tp], R_A + p * (NTP - 1) + d - 1, t_peer[d])

    def attended_wait(p):
        for d in range(1, NTP):
            arrived(att_all.at[p, (tp + NTP - d) % NTP], R_A + p * (NTP - 1) + d - 1)

    def log_weights():
        levels = jnp.transpose(lw_s[...])[0:8, :]
        high = levels.astype(BF16)
        rest = levels - high.astype(F32)
        mid = rest.astype(BF16)
        low = (rest - mid.astype(F32)).astype(BF16)
        natural = dot(high, perm[0]) + dot(mid, perm[0]) + dot(low, perm[0])
        lw_out[...] = natural[0:4, :]

    def project():
        def step(c, squares):
            cols = pl.ds(pl.multiple_of(c * 512, 512), 512)
            total = None
            for g in range(NTP):
                a = jnp.concatenate([att_all[0, g], att_all[1, g]], axis=1)
                part = dot(a, wo_v[g, :, cols]).astype(BF16).astype(F32)
                total = part if total is None else total + part
            sum_s[:, cols] = total
            return squares + jnp.sum(total * total, axis=-1, keepdims=True)

        squares = lax.fori_loop(0, 4, step, jnp.zeros((OUT_ROWS, 1), F32))
        scale = lax.rsqrt(squares / D + EPS)
        out[...] = (sum_s[...] * scale * post[...]).astype(BF16)

    weights_y_send(0)
    wo_send()
    weights_y_send(1)
    norm()
    weights_y_wait(0)
    weights_z_send(0)
    weights_y_wait(1)
    permutation()
    permute()
    weights_z_step(0, 0)
    tables()
    biases()
    weights_z_step(0, 1)
    queries()
    weights_z_step(0, 2)
    weights_z_send(1)
    wo_step(0)
    weights_z_step(0, 3)
    keys_values(0)
    halo_send(0)
    weights_z_step(1, 0)
    near(0, 1, 4)
    weights_z_step(1, 1)
    halo_step(0, 1)
    near(0, 0, 1)
    weights_z_step(1, 2)
    far(0, (0, 1))
    weights_z_step(1, 3)
    keys_values(1)
    halo_send(1)
    halo_step(0, 2)
    wo_step(1)
    near(1, 1, 4)
    halo_step(0, 3)
    far(0, (2, 3))
    halo_step(1, 1)
    wo_step(2)
    near(1, 0, 1)
    far(1, (0, 1))
    halo_step(0, 4)
    far(0, (4,))
    finish(0)
    halo_step(1, 2)
    halo_step(1, 3)
    far(1, (2, 3))
    wo_sibling_wait()
    attended_wait(0)
    halo_step(1, 4)
    far(1, (4,))
    finish(1)
    log_weights()
    attended_wait(1)
    project()
    for copy in sends:
        copy.wait_send()


def body(hidden_in, pre_gain, query_proj, key_proj, value_proj, out_proj, post_gain):
    half = np.arange(HEAD_DIM // 2, dtype=np.float32) * np.float32(2.0) / np.float32(HEAD_DIM)
    freq = np.tile(np.power(np.float64(ROPE_BASE), -half.astype(np.float64)).astype(np.float32), 4).reshape(1, 128)
    any_spec = pl.BlockSpec(memory_space=pl.ANY)
    vmem = pl.BlockSpec(memory_space=pltpu.VMEM)
    return pl.pallas_call(
        kernel,
        out_shape=(jax.ShapeDtypeStruct((OUT_ROWS, D), BF16), jax.ShapeDtypeStruct((4, ROWS), F32)),
        in_specs=[any_spec, vmem, vmem, any_spec, any_spec, any_spec, any_spec, vmem],
        out_specs=(vmem, vmem),
        scratch_shapes=[
            pltpu.VMEM((ROWS, D), BF16),
            pltpu.VMEM((ROWS, D), BF16),
            pltpu.VMEM((D, WIDTH), BF16),
            pltpu.VMEM((2, D, WIDTH), BF16),
            pltpu.VMEM((NTP, WIDTH, D), BF16),
            pltpu.VMEM((SLOTS, 2, 2, ROWS, 128), BF16),
            pltpu.VMEM((2, 4, 256, 128), BF16),
            pltpu.VMEM((2, 4, 256, 128), F32),
            pltpu.VMEM((2, 4, 256, 128), F32),
            pltpu.VMEM((2, 4, 256, 128), F32),
            pltpu.VMEM((ROWS, 128), BF16),
            pltpu.VMEM((2, ROWS, 128), BF16),
            pltpu.VMEM((2, NTP, OUT_ROWS, 128), BF16),
            pltpu.VMEM((ROWS, 128), F32),
            pltpu.VMEM((ROWS, 128), F32),
            pltpu.VMEM((ROWS, 128), F32),
            pltpu.VMEM((128, SLOTS * 128), F32),
            pltpu.VMEM((2, 128, 256), F32),
            pltpu.VMEM((2, ROWS, ROWS), BF16),
            pltpu.VMEM((OUT_ROWS, D), F32),
            pltpu.SemaphoreType.DMA((7,)),
            pltpu.SemaphoreType.DMA((N_SEND,)),
            pltpu.SemaphoreType.DMA((R_END,)),
        ],
        compiler_params=pltpu.CompilerParams(
            collective_id=0, has_side_effects=True, vmem_limit_bytes=60 * 1024 * 1024
        ),
        name="layer",
    )(
        hidden_in, pre_gain.reshape(1, D), jnp.asarray(freq), query_proj, key_proj, value_proj, out_proj,
        post_gain.reshape(1, D),
    )


def solution(mesh):
    placed = (P("sp", None), P(), P(None, "tp"), P("sp", "tp"), P("sp", "tp"), P("tp", None), P())
    return jax.shard_map(
        body,
        mesh=mesh,
        in_specs=placed,
        out_specs=(P(("sp", "tp"), None), P("tp", "sp")),
        check_vma=False,
    )
```

time: 263 us -> 146 us (0.56)
  the two profiles are of different devices: /device:TPU:1 before, /device:TPU:33 now
where the time goes in v1:
time: 146 us
  Pallas kernels  143 us (98%)
  local copies, waits for them, and re-layouts  2.96 us (2%)
    pallas_call x1, Pallas kernels, body(): pl.pallas_call(kernel, out_shape=(jax.ShapeDtypeStruct((OUT_ROWS, D), BF1...  143 us
    unnamed x2, local copies, waits for them, and re-layouts  2.96 us

profile of v1, /device:TPU:33, one launch (start us, length us, event | category | flops | bytes accessed | tf_op | source)
XLA Modules:
  0.0 146.2 jit_solution(11299137864116140815)
XLA Ops:
  0.6 142.6 %layer.1 = (bf16[64,2048]{1,0:T(8,128)(2,1)}, f32[4,512]{1,0:T(4,128)}) custom-call(bf16[512,2048]{1,0:T(8,128)(2,1)} %hid.1, f32[1,2048]{1,0:T(1,128)} %bitcast.2, f32[1,128]{1,0:T(1,128)} %constant.2.clone.freq, bf16[2048,256]{1,0:T(8,128)(2,1)} %wq.1, bf16[32,256]{1,0:T(8,128)(2,1)} %wk.1, bf16[32,256]{1,0:T(8,128)(2,1)} %wv.1, bf16[256,2048]{1,0:T(8,128)(2,1)} %wo.1, ...), custom_call_target="tpu_custom_call" | custom-call | tf_op jit(solution)/shard_map/layer/pallas_call | solution.py:460
  143.2 1.7 %copy.12 = bf16[64,2048]{1,0:T(8,128)(2,1)} copy(bf16[64,2048]{1,0:T(8,128)(2,1)} %get-tuple-element.4) | data formatting | bytes 524288
  144.9 1.3 copy.13

commit v2 on v1

--- a/solution.py
+++ b/solution.py
@@ -33,13 +33,16 @@
 NT = (((1,), (1,)), ((), ()))
 NN = (((1,), (0,)), ((), ()))
 
-R_WY = 0
-R_WZ = R_WY + 2 * (NY - 1)
-R_X = R_WZ + 2 * 2 * 2 * 4
+AHEAD_ROWS = 320
+
+R_WD = 0
+R_WR = R_WD + 2 * 2 * 7
+R_X = R_WR + 2 * 2 * 2 * 2 * 4
 R_H = R_X + 16
-R_A = R_H + 2 * SLOTS
+R_M = R_H + 2 * SLOTS
+R_A = R_M + 2 * SLOTS
 R_END = R_A + 2 * (NTP - 1)
-N_SEND = 110
+N_SEND = 140
 
 
 def dot(a, b, dims=NN):
@@ -53,7 +56,7 @@
 def kernel(
     hid, gain, freq, wq, wk, wv, wo, post,
     out, lw_out,
-    hid_v, np_v, wq_v, w_v, wo_v, kv, q_s, st_o, st_m, st_l, att_p, att_n, att_all, lw_s,
+    hid_v, np_v, wq_v, w_v, wo_v, kv, passing, q_s, st_o, st_m, st_l, att_p, att_n, att_all, lw_s,
     cos_s, sin_s, bias_c, bias_n, perm, sum_s, lsem, ssem, rsem,
 ):
     sp = lax.axis_index("sp")
@@ -77,21 +80,23 @@
         ).wait_recv()
 
     y_peer = [(z * NY + (y + d) % NY, tp) for d in range(NY)]
-    z_up = (((z + 1) % NZ) * NY + y, tp)
-    z_down = (((z + NZ - 1) % NZ) * NY + y, tp)
+    z_peer = [(((z + d) % NZ) * NY + y, tp) for d in range(NZ)]
     ahead = ((sp + 1) % NSP, tp)
     behind = ((sp + NSP - 1) % NSP, tp)
+    relay_of_me = y_peer[NY - 3]
+    relay_to = ((z * NY + (y + 3) % NY + 4) % NSP, tp)
+    source = (sp + NSP - 4) % NSP
+    relay_from = ((source // NY) * NY + (source % NY + NY - 3) % NY, tp)
     t_peer = [(sp, (tp + d) % NTP) for d in range(NTP)]
     x_right = (sp, (tp + 2) % NTP)
     x_left = (sp, (tp + NTP - 2) % NTP)
     sibling = (sp, x * 2 + (1 - core))
 
-    wrow = pl.ds(pl.multiple_of(sp * 32, 32), 32)
     local = [
-        pltpu.make_async_copy(wk.at[:, 0:128], w_v.at[0, wrow, 0:128], lsem.at[0]),
-        pltpu.make_async_copy(wv.at[:, 0:128], w_v.at[0, wrow, 128:256], lsem.at[1]),
-        pltpu.make_async_copy(wk.at[:, 128:256], w_v.at[1, wrow, 0:128], lsem.at[2]),
-        pltpu.make_async_copy(wv.at[:, 128:256], w_v.at[1, wrow, 128:256], lsem.at[3]),
+        pltpu.make_async_copy(w.at[:, p * 128 : (p + 1) * 128], w_v.at[i, p, z, y], lsem.at[2 * p + i])
+        for p in range(2)
+        for i, w in enumerate((wk, wv))
+    ] + [
         pltpu.make_async_copy(wo, wo_v.at[tp], lsem.at[4]),
         pltpu.make_async_copy(hid, hid_v, lsem.at[5]),
         pltpu.make_async_copy(wq, wq_v, lsem.at[6]),
@@ -100,47 +105,52 @@
         copy.start()
 
     barrier = pltpu.get_barrier_semaphore()
-    partners = y_peer[1:] + t_peer[1:] + [z_up, z_down, ahead, behind]
+    partners = y_peer[1:] + z_peer[1:] + t_peer[1:] + [ahead, behind, relay_to, relay_from]
     for dev in partners:
         pl.semaphore_signal(barrier, inc=1, device_id=dev, device_id_type=MESH)
     pl.semaphore_wait(barrier, len(partners))
 
-    def weights_y_send(p):
-        local[2 * p].wait()
-        local[2 * p + 1].wait()
-        for d in range(1, NY):
-            start(w_v.at[p, wrow], w_v.at[p, wrow], R_WY + p * (NY - 1) + d - 1, y_peer[d])
-
-    def weights_y_wait(p):
-        for d in range(1, NY):
-            row = (z * NY + (y + NY - d) % NY) * 32
-            arrived(w_v.at[p, pl.ds(pl.multiple_of(row, 32), 32)], R_WY + p * (NY - 1) + d - 1)
-
-    def z_rows(zz, half):
-        return pl.ds(pl.multiple_of(zz * 256 + half * 128, 128), 128)
-
-    def z_sem(p, half, direction, hop):
-        return R_WZ + ((p * 2 + half) * 2 + direction) * 4 + hop
-
-    def z_hops(half, direction):
-        return 4 if half == direction else 3
-
-    def weights_z_send(p):
+    def weights_send(p):
+        for i, peer in enumerate((y_peer, z_peer)):
+            local[2 * p + i].wait()
+            part = w_v.at[i, p, z, y]
+            for d in range(1, 8):
+                start(part, part, R_WD + (i * 2 + p) * 7 + d - 1, peer[d])
+
+    def weights_wait(p):
+        for d in range(1, 8):
+            arrived(w_v.at[0, p, z, (y + NY - d) % NY], R_WD + p * 7 + d - 1)
+            arrived(w_v.at[1, p, (z + NZ - d) % NZ, y], R_WD + (2 + p) * 7 + d - 1)
+
+    def relay_part(i, p, at, half):
+        piece = pl.ds(half * 4, 4)
+        return w_v.at[0, p, at, piece] if i == 0 else w_v.at[1, p, piece, at]
+
+    def relay_sem(i, p, half, direction, hop):
+        return R_WR + (((i * 2 + p) * 2 + half) * 2 + direction) * 4 + hop
+
+    def relay_dev(i, direction):
+        peer = z_peer if i == 0 else y_peer
+        return peer[1] if direction == 0 else peer[7]
+
+    def relay_send(p):
         for half in range(2):
-            part = w_v.at[p, z_rows(z, half)]
-            start(part, part, z_sem(p, half, 0, 0), z_up)
-            start(part, part, z_sem(p, half, 1, 0), z_down)
-
-    def weights_z_step(p, hop):
+            for i, at in enumerate((z, y)):
+                part = relay_part(i, p, at, half)
+                for direction in range(2):
+                    start(part, part, relay_sem(i, p, half, direction, 0), relay_dev(i, direction))
+
+    def relay_step(p, hop):
         for half in range(2):
-            for direction in range(2):
-                hops = z_hops(half, direction)
-                if hop < hops:
-                    zz = (z + NZ - 1 - hop) % NZ if direction == 0 else (z + 1 + hop) % NZ
-                    part = w_v.at[p, z_rows(zz, half)]
-                    arrived(part, z_sem(p, half, direction, hop))
-                    if hop + 1 < hops:
-                        start(part, part, z_sem(p, half, direction, hop + 1), z_up if direction == 0 else z_down)
+            for i, at in enumerate((z, y)):
+                for direction in range(2):
+                    hops = 4 if half == direction else 3
+                    if hop < hops:
+                        owner = (at + 7 - hop) % 8 if direction == 0 else (at + 1 + hop) % 8
+                        part = relay_part(i, p, owner, half)
+                        arrived(part, relay_sem(i, p, half, direction, hop))
+                        if hop + 1 < hops:
+                            start(part, part, relay_sem(i, p, half, direction, hop + 1), relay_dev(i, direction))
 
     def wo_part(delta, part):
         group = wo_v.at[(tp + delta) % NTP]
@@ -188,13 +198,29 @@
         arrived(part_of(4, 0), R_X + 11)
         arrived(part_of(4, 1), R_X + 12)
 
+    def up_part(k, p):
+        return kv.at[k, p, :, 0:AHEAD_ROWS]
+
+    def down_part(k, p):
+        return kv.at[k, p, :, AHEAD_ROWS:ROWS]
+
     def halo_send(p):
-        start(kv.at[0, p], kv.at[1, p], R_H + p * SLOTS + 1, ahead)
-
-    def halo_step(p, k):
-        arrived(kv.at[k, p], R_H + p * SLOTS + k)
+        start(up_part(0, p), up_part(1, p), R_H + p * SLOTS + 1, ahead)
+        start(down_part(0, p), passing.at[p], R_M + p * SLOTS, relay_of_me)
+
+    def up(p, k):
+        arrived(up_part(k, p), R_H + p * SLOTS + k)
         if k < SLOTS - 1:
-            start(kv.at[k, p], kv.at[k + 1, p], R_H + p * SLOTS + k + 1, ahead)
+            start(up_part(k, p), up_part(k + 1, p), R_H + p * SLOTS + k + 1, ahead)
+
+    def down(p, k):
+        if k == 0:
+            arrived(passing.at[p], R_M + p * SLOTS)
+            start(passing.at[p], down_part(4, p), R_M + p * SLOTS + 4, relay_to)
+        else:
+            arrived(down_part(k, p), R_M + p * SLOTS + k)
+            if k > 1:
+                start(down_part(k, p), down_part(k - 1, p), R_M + p * SLOTS + k - 1, behind)
 
     lane = lax.broadcasted_iota(jnp.int32, (1, 128), 1)
     first_head = lane < 64
@@ -282,9 +308,11 @@
         lax.fori_loop(0, 4, step, 0)
 
     def keys_values(p):
+        weights = jnp.concatenate([w_v[i, p].reshape(D, 128) for i in range(2)], axis=1)
+
         def step(r, _):
             rows = pl.ds(pl.multiple_of(r * 128, 128), 128)
-            both = dot(np_v[rows, :], w_v[p])
+            both = dot(np_v[rows, :], weights)
             kv[0, p, 0, rows, :] = rotate(both[:, 0:128], rows)
             kv[0, p, 1, rows, :] = both[:, 128:256].astype(BF16)
             return 0
@@ -295,13 +323,18 @@
         def step(b, _):
             slot = (3 - b) // 3
             before = (b + 3) % 4
+            state = [(r, pl.ds(pl.multiple_of(h * 128 + b * 32, 32), 32)) for h in range(2) for r in range(4)]
+
+            def gathered(ref):
+                return jnp.concatenate([ref[p, r, at, :] for r, at in state], axis=0)
+
+            def scattered(ref, value):
+                for i, (r, at) in enumerate(state):
+                    ref[p, r, at, :] = value[i * 32 : (i + 1) * 32]
 
             def part(r, base):
                 return pl.ds(pl.multiple_of(base + r * 128, 32), 32)
 
-            q = jnp.concatenate(
-                [q_s[p, r, pl.ds(pl.multiple_of(h * 128 + b * 32, 32), 32), :] for h in range(2) for r in range(4)], axis=0
-            )
             k, v = (
                 jnp.concatenate(
                     [kv[slot, p, w, part(r, before * 32), :] for r in range(4)]
@@ -310,45 +343,40 @@
                 )
                 for w in range(2)
             )
-            bias = bias_n[jnp.minimum(b, 1)]
-            s = dot(q, k, NT) * SCALE2 + jnp.concatenate([bias, bias], axis=0)
-            m = jnp.max(s, axis=-1, keepdims=True)
-            e = jnp.exp2(s - m)
-            total = jnp.sum(e, axis=-1, keepdims=True)
-            o = dot(e.astype(BF16), v)
-            m = jnp.broadcast_to(m, o.shape)
-            total = jnp.broadcast_to(total, o.shape)
-            for h in range(2):
-                for r in range(4):
-                    at = pl.ds(pl.multiple_of(h * 128 + b * 32, 32), 32)
-                    piece = slice(h * 128 + r * 32, h * 128 + r * 32 + 32)
-                    st_o[p, r, at, :] = o[piece]
-                    st_m[p, r, at, :] = m[piece]
-                    st_l[p, r, at, :] = total[piece]
+            o, m, total = update(
+                gathered(q_s), k, v, bias_n[jnp.minimum(b, 1)], (gathered(st_o), gathered(st_m), gathered(st_l))
+            )
+            scattered(st_o, o)
+            scattered(st_m, m)
+            scattered(st_l, total)
             return 0
 
         lax.fori_loop(first, last, step, 0)
 
-    def far(p, slots):
+    def update(q, k, v, bias, state):
+        s = dot(q, k, NT) * SCALE2 + jnp.concatenate([bias, bias], axis=0)
+        m = jnp.broadcast_to(jnp.max(s, axis=-1, keepdims=True), q.shape)
+        if state is not None:
+            m = jnp.maximum(m, state[1])
+        e = jnp.exp2(s - jnp.concatenate([m] * (s.shape[1] // 128), axis=1))
+        total = jnp.broadcast_to(jnp.sum(e, axis=-1, keepdims=True), q.shape)
+        o = dot(e.astype(BF16), v)
+        if state is not None:
+            decay = jnp.exp2(state[1] - m)
+            total = state[2] * decay + total
+            o = state[0] * decay + o
+        return o, m, total
+
+    def far(p, first, last, slots):
         def step(r, _):
             rows = pl.ds(pl.multiple_of(r * 128, 128), 128)
-            k, v = (
-                jnp.concatenate([kv[s, p, w, rows, :] for s in slots], axis=0) if len(slots) > 1 else kv[slots[0], p, w, rows, :]
-                for w in range(2)
-            )
+            k, v = (jnp.concatenate([kv[s, p, w, rows, :] for s in slots], axis=0) for w in range(2))
             bias = bias_c[:, slots[0] * 128 : (slots[-1] + 1) * 128]
-            s = dot(q_s[p, r], k, NT) * SCALE2 + jnp.concatenate([bias, bias], axis=0)
-            m_old = st_m[p, r]
-            m = jnp.maximum(m_old, jnp.broadcast_to(jnp.max(s, axis=-1, keepdims=True), m_old.shape))
-            wide = m if len(slots) == 1 else jnp.concatenate([m] * len(slots), axis=1)
-            e = jnp.exp2(s - wide)
-            decay = jnp.exp2(m_old - m)
-            st_l[p, r] = st_l[p, r] * decay + jnp.broadcast_to(jnp.sum(e, axis=-1, keepdims=True), m.shape)
-            st_o[p, r] = st_o[p, r] * decay + dot(e.astype(BF16), v)
-            st_m[p, r] = m
+            state = None if slots[0] == 0 else (st_o[p, r], st_m[p, r], st_l[p, r])
+            st_o[p, r], st_m[p, r], st_l[p, r] = update(q_s[p, r], k, v, bias, state)
             return 0
 
-        lax.fori_loop(0, 4, step, 0)
+        lax.fori_loop(first, last, step, 0)
 
     def finish(p):
         for r in range(4):
@@ -395,56 +423,71 @@
         scale = lax.rsqrt(squares / D + EPS)
         out[...] = (sum_s[...] * scale * post[...]).astype(BF16)
 
-    weights_y_send(0)
+    weights_send(0)
+    weights_send(1)
     wo_send()
-    weights_y_send(1)
     norm()
-    weights_y_wait(0)
-    weights_z_send(0)
-    weights_y_wait(1)
     permutation()
+    weights_wait(0)
+    relay_send(0)
+    weights_wait(1)
+    relay_send(1)
     permute()
-    weights_z_step(0, 0)
+    relay_step(0, 0)
+    relay_step(1, 0)
     tables()
     biases()
-    weights_z_step(0, 1)
+    relay_step(0, 1)
+    relay_step(1, 1)
     queries()
-    weights_z_step(0, 2)
-    weights_z_send(1)
+    relay_step(0, 2)
+    relay_step(1, 2)
     wo_step(0)
-    weights_z_step(0, 3)
+    relay_step(0, 3)
     keys_values(0)
     halo_send(0)
-    weights_z_step(1, 0)
-    near(0, 1, 4)
-    weights_z_step(1, 1)
-    halo_step(0, 1)
-    near(0, 0, 1)
-    weights_z_step(1, 2)
-    far(0, (0, 1))
-    weights_z_step(1, 3)
+    relay_step(1, 3)
     keys_values(1)
     halo_send(1)
-    halo_step(0, 2)
+    far(0, 0, 4, (0,))
+    near(0, 1, 4)
+    up(0, 1)
+    far(1, 0, 4, (0,))
+    down(0, 0)
+    up(1, 1)
+    near(1, 1, 4)
     wo_step(1)
-    near(1, 1, 4)
-    halo_step(0, 3)
-    far(0, (2, 3))
-    halo_step(1, 1)
+    down(1, 0)
+    up(0, 2)
+    far(0, 0, 2, (1, 2))
+    down(0, 4)
+    up(1, 2)
+    far(1, 0, 2, (1, 2))
+    down(1, 4)
+    down(0, 3)
+    up(0, 3)
     wo_step(2)
+    down(1, 3)
+    far(0, 3, 4, (3, 4))
+    up(1, 3)
+    far(1, 3, 4, (3, 4))
+    down(0, 2)
+    up(0, 4)
+    far(0, 0, 2, (3, 4))
+    down(1, 2)
+    far(0, 2, 3, (3, 4))
+    down(0, 1)
+    far(0, 2, 4, (1, 2))
+    near(0, 0, 1)
+    finish(0)
+    up(1, 4)
+    far(1, 0, 3, (3, 4))
+    down(1, 1)
+    far(1, 2, 4, (1, 2))
     near(1, 0, 1)
-    far(1, (0, 1))
-    halo_step(0, 4)
-    far(0, (4,))
-    finish(0)
-    halo_step(1, 2)
-    halo_step(1, 3)
-    far(1, (2, 3))
+    finish(1)
     wo_sibling_wait()
     attended_wait(0)
-    halo_step(1, 4)
-    far(1, (4,))
-    finish(1)
     log_weights()
     attended_wait(1)
     project()
@@ -466,9 +509,10 @@
             pltpu.VMEM((ROWS, D), BF16),
             pltpu.VMEM((ROWS, D), BF16),
             pltpu.VMEM((D, WIDTH), BF16),
-            pltpu.VMEM((2, D, WIDTH), BF16),
+            pltpu.VMEM((2, 2, NZ, NY, D // NSP, 128), BF16),
             pltpu.VMEM((NTP, WIDTH, D), BF16),
             pltpu.VMEM((SLOTS, 2, 2, ROWS, 128), BF16),
+            pltpu.VMEM((2, 2, ROWS - AHEAD_ROWS, 128), BF16),
             pltpu.VMEM((2, 4, 256, 128), BF16),
             pltpu.VMEM((2, 4, 256, 128), F32),
             pltpu.VMEM((2, 4, 256, 128), F32),

time: 146 us -> 89.6 us (0.61)
  the two profiles are of different devices: /device:TPU:33 before, /device:TPU:1 now
where the time goes in v2:
time: 89.6 us; the launch traced here: 89.4 us
  Pallas kernels  85.7 us (96%)
  local copies, waits for them, and re-layouts  2.96 us (3%)
    pallas_call x1, Pallas kernels, body(): pl.pallas_call(kernel, out_shape=(jax.ShapeDtypeStruct((OUT_ROWS, D), BF1...  85.7 us
    unnamed x2, local copies, waits for them, and re-layouts  2.96 us

profile of v2, /device:TPU:1, one launch (start us, length us, event | category | flops | bytes accessed | tf_op | source)
XLA Modules:
  0.0 89.4 jit_solution(5985833154345542914)
XLA Ops:
  0.6 85.7 %layer.1 = (bf16[64,2048]{1,0:T(8,128)(2,1)}, f32[4,512]{1,0:T(4,128)}) custom-call(bf16[512,2048]{1,0:T(8,128)(2,1)} %hid.1, f32[1,2048]{1,0:T(1,128)} %bitcast.2, f32[1,128]{1,0:T(1,128)} %constant.2.clone.freq, bf16[2048,256]{1,0:T(8,128)(2,1)} %wq.1, bf16[32,256]{1,0:T(8,128)(2,1)} %wk.1, bf16[32,256]{1,0:T(8,128)(2,1)} %wv.1, bf16[256,2048]{1,0:T(8,128)(2,1)} %wo.1, ...), custom_call_target="tpu_custom_call" | custom-call | tf_op jit(solution)/shard_map/layer/pallas_call | solution.py:503
  86.4 1.7 %copy.12 = bf16[64,2048]{1,0:T(8,128)(2,1)} copy(bf16[64,2048]{1,0:T(8,128)(2,1)} %get-tuple-element.4) | data formatting | bytes 524288
  88.1 1.3 %copy.13 = f32[4,512]{1,0:T(4,128)} copy(f32[4,512]{1,0:T(4,128)} %get-tuple-element.5) | data formatting | bytes 16384

commit v3 on v2

--- a/solution.py
+++ b/solution.py
@@ -26,6 +26,7 @@
 NEG = -1e30
 SCALE2 = math.log2(math.e) / 8.0
 LN2 = math.log(2.0)
+BIG = 512
 F32 = jnp.float32
 BF16 = jnp.bfloat16
 MESH = pl.DeviceIdType.MESH
@@ -54,9 +55,9 @@
 
 
 def kernel(
-    hid, gain, freq, wq, wk, wv, wo, post,
-    out, lw_out,
-    hid_v, np_v, wq_v, w_v, wo_v, kv, passing, q_s, st_o, st_m, st_l, att_p, att_n, att_all, lw_s,
+    hid, gain_h, freq_h, wq, wk, wv, wo, post_h,
+    out_h, lw_h,
+    gain, freq, post, out, lw_out, hid_v, np_v, wq_v, w_v, wo_v, kv, passing, q_s, st_o, st_m, st_l, att_p, att_n, att_all, lw_s,
     cos_s, sin_s, bias_c, bias_n, perm, sum_s, lsem, ssem, rsem,
 ):
     sp = lax.axis_index("sp")
@@ -100,9 +101,14 @@
         pltpu.make_async_copy(wo, wo_v.at[tp], lsem.at[4]),
         pltpu.make_async_copy(hid, hid_v, lsem.at[5]),
         pltpu.make_async_copy(wq, wq_v, lsem.at[6]),
+        pltpu.make_async_copy(gain_h, gain, lsem.at[7]),
+        pltpu.make_async_copy(freq_h, freq, lsem.at[8]),
+        pltpu.make_async_copy(post_h, post, lsem.at[9]),
     ]
     for copy in local:
         copy.start()
+
+    lw_copy = pltpu.make_async_copy(lw_out, lw_h, lsem.at[10])
 
     barrier = pltpu.get_barrier_semaphore()
     partners = y_peer[1:] + z_peer[1:] + t_peer[1:] + [ahead, behind, relay_to, relay_from]
@@ -228,6 +234,7 @@
 
     def norm():
         local[5].wait()
+        local[7].wait()
 
         def step(i, _):
             rows = pl.ds(pl.multiple_of(i * 32, 32), 32)
@@ -253,9 +260,10 @@
                 np_v[rows, c * 512 : (c + 1) * 512] = dot(perm[0, rows, :], hid_v[:, c * 512 : (c + 1) * 512]).astype(BF16)
             return 0
 
-        lax.fori_loop(0, 4, step, 0)
+        lax.fori_loop(0, 4, step, 0, unroll=2)
 
     def tables():
+        local[8].wait()
         token = token_of(lax.broadcasted_iota(jnp.int32, (ROWS, 128), 0))
         angle = (sp * ROWS + token).astype(F32) * freq[...]
         cos_s[...] = jnp.cos(angle)
@@ -295,29 +303,24 @@
     def queries():
         local[6].wait()
 
-        def step(r, _):
-            rows = pl.ds(pl.multiple_of(r * 128, 128), 128)
-            q = dot(np_v[rows, :], wq_v[...])
-            for p in range(2):
-                turned = rotate(q[:, p * 128 : (p + 1) * 128], rows)
-                zero = jnp.zeros_like(turned)
-                q_s[p, r, 0:128, :] = jnp.where(first_head, turned, zero)
-                q_s[p, r, 128:256, :] = jnp.where(first_head, zero, turned)
-            return 0
-
-        lax.fori_loop(0, 4, step, 0)
+        for r0 in range(0, ROWS, BIG):
+            q = dot(np_v[r0 : r0 + BIG, :], wq_v[...])
+            for r in range(BIG // 128):
+                rows = slice(r0 + r * 128, r0 + r * 128 + 128)
+                for p in range(2):
+                    turned = rotate(q[r * 128 : r * 128 + 128, p * 128 : (p + 1) * 128], rows)
+                    zero = jnp.zeros_like(turned)
+                    q_s[p, r0 // 128 + r, 0:128, :] = jnp.where(first_head, turned, zero)
+                    q_s[p, r0 // 128 + r, 128:256, :] = jnp.where(first_head, zero, turned)
 
     def keys_values(p):
         weights = jnp.concatenate([w_v[i, p].reshape(D, 128) for i in range(2)], axis=1)
 
-        def step(r, _):
-            rows = pl.ds(pl.multiple_of(r * 128, 128), 128)
+        for r0 in range(0, ROWS, BIG):
+            rows = slice(r0, r0 + BIG)
             both = dot(np_v[rows, :], weights)
             kv[0, p, 0, rows, :] = rotate(both[:, 0:128], rows)
             kv[0, p, 1, rows, :] = both[:, 128:256].astype(BF16)
-            return 0
-
-        lax.fori_loop(0, 4, step, 0)
 
     def near(p, first, last):
         def step(b, _):
@@ -351,7 +354,7 @@
             scattered(st_l, total)
             return 0
 
-        lax.fori_loop(first, last, step, 0)
+        lax.fori_loop(first, last, step, 0, unroll=True)
 
     def update(q, k, v, bias, state):
         s = dot(q, k, NT) * SCALE2 + jnp.concatenate([bias, bias], axis=0)
@@ -376,7 +379,7 @@
             st_o[p, r], st_m[p, r], st_l[p, r] = update(q_s[p, r], k, v, bias, state)
             return 0
 
-        lax.fori_loop(first, last, step, 0)
+        lax.fori_loop(first, last, step, 0, unroll=True)
 
     def finish(p):
         for r in range(4):
@@ -407,6 +410,7 @@
         low = (rest - mid.astype(F32)).astype(BF16)
         natural = dot(high, perm[0]) + dot(mid, perm[0]) + dot(low, perm[0])
         lw_out[...] = natural[0:4, :]
+        lw_copy.start()
 
     def project():
         def step(c, squares):
@@ -421,25 +425,29 @@
 
         squares = lax.fori_loop(0, 4, step, jnp.zeros((OUT_ROWS, 1), F32))
         scale = lax.rsqrt(squares / D + EPS)
+        local[9].wait()
         out[...] = (sum_s[...] * scale * post[...]).astype(BF16)
+        out_copy = pltpu.make_async_copy(out, out_h, lsem.at[11])
+        out_copy.start()
+        lw_copy.wait()
+        out_copy.wait()
 
     weights_send(0)
     weights_send(1)
     wo_send()
     norm()
     permutation()
+    permute()
     weights_wait(0)
     relay_send(0)
     weights_wait(1)
     relay_send(1)
-    permute()
+    tables()
     relay_step(0, 0)
     relay_step(1, 0)
-    tables()
     biases()
     relay_step(0, 1)
     relay_step(1, 1)
-    queries()
     relay_step(0, 2)
     relay_step(1, 2)
     wo_step(0)
@@ -449,6 +457,7 @@
     relay_step(1, 3)
     keys_values(1)
     halo_send(1)
+    queries()
     far(0, 0, 4, (0,))
     near(0, 1, 4)
     up(0, 1)
@@ -495,17 +504,27 @@
         copy.wait_send()
 
 
+def hand_over(out_in, lw_in, out, lw_out):
+    out[...] = out_in[...]
+    lw_out[...] = lw_in[...]
+
+
 def body(hidden_in, pre_gain, query_proj, key_proj, value_proj, out_proj, post_gain):
     half = np.arange(HEAD_DIM // 2, dtype=np.float32) * np.float32(2.0) / np.float32(HEAD_DIM)
     freq = np.tile(np.power(np.float64(ROPE_BASE), -half.astype(np.float64)).astype(np.float32), 4).reshape(1, 128)
     any_spec = pl.BlockSpec(memory_space=pl.ANY)
     vmem = pl.BlockSpec(memory_space=pltpu.VMEM)
-    return pl.pallas_call(
+    results = pl.pallas_call(
         kernel,
         out_shape=(jax.ShapeDtypeStruct((OUT_ROWS, D), BF16), jax.ShapeDtypeStruct((4, ROWS), F32)),
-        in_specs=[any_spec, vmem, vmem, any_spec, any_spec, any_spec, any_spec, vmem],
-        out_specs=(vmem, vmem),
+        in_specs=[any_spec] * 8,
+        out_specs=(any_spec, any_spec),
         scratch_shapes=[
+            pltpu.VMEM((1, D), F32),
+            pltpu.VMEM((1, 128), F32),
+            pltpu.VMEM((1, D), F32),
+            pltpu.VMEM((OUT_ROWS, D), BF16),
+            pltpu.VMEM((4, ROWS), F32),
             pltpu.VMEM((ROWS, D), BF16),
             pltpu.VMEM((ROWS, D), BF16),
             pltpu.VMEM((D, WIDTH), BF16),
@@ -527,7 +546,7 @@
             pltpu.VMEM((2, 128, 256), F32),
             pltpu.VMEM((2, ROWS, ROWS), BF16),
             pltpu.VMEM((OUT_ROWS, D), F32),
-            pltpu.SemaphoreType.DMA((7,)),
+            pltpu.SemaphoreType.DMA((12,)),
             pltpu.SemaphoreType.DMA((N_SEND,)),
             pltpu.SemaphoreType.DMA((R_END,)),
         ],
@@ -539,6 +558,13 @@
         hidden_in, pre_gain.reshape(1, D), jnp.asarray(freq), query_proj, key_proj, value_proj, out_proj,
         post_gain.reshape(1, D),
     )
+    return pl.pallas_call(
+        hand_over,
+        out_shape=(jax.ShapeDtypeStruct((OUT_ROWS, D), BF16), jax.ShapeDtypeStruct((4, ROWS), F32)),
+        in_specs=[vmem, vmem],
+        out_specs=(vmem, vmem),
+        name="hand_over",
+    )(*results)
 
 
 def solution(mesh):

time: 89.6 us -> 85.2 us (0.951)
  local copies, waits for them, and re-layouts: 2.96 us -> 0 us
  Pallas kernels: 85.7 us -> 84.4 us
    pallas_call x1, Pallas kernels: 85.7 us -> 82.7 us  [body(): pl.pallas_call(kernel, out_shape=(jax.ShapeDtypeStruct((OUT_ROWS, D), BF1...]
    unnamed x2 -> x0, local copies, waits for them, and re-layouts: 2.96 us -> none
    pallas_call x0 -> x1, Pallas kernels: none -> 1.68 us  [body(): pl.pallas_call(hand_over, out_shape=(jax.ShapeDtypeStruct((OUT_ROWS, D),...]
where the time goes in v3:
time: 85.2 us; the launch traced here: 85.1 us
  Pallas kernels  84.4 us (99%)
    pallas_call x1, Pallas kernels, body(): pl.pallas_call(kernel, out_shape=(jax.ShapeDtypeStruct((OUT_ROWS, D), BF1...  82.7 us

profile of v3, /device:TPU:1, one launch (start us, length us, event | category | flops | bytes accessed | tf_op | source)
XLA Modules:
  0.0 85.1 jit_solution(4318399136185104273)
XLA Ops:
  0.6 82.7 %layer.1 = (bf16[64,2048]{1,0:T(8,128)(2,1)}, f32[4,512]{1,0:T(4,128)}) custom-call(bf16[512,2048]{1,0:T(8,128)(2,1)} %hid.1, f32[1,2048]{1,0:T(1,128)} %bitcast.2, f32[1,128]{1,0:T(1,128)} %constant.2.clone.freq_h, bf16[2048,256]{1,0:T(8,128)(2,1)} %wq.1, bf16[32,256]{1,0:T(8,128)(2,1)} %wk.1, bf16[32,256]{1,0:T(8,128)(2,1)} %wv.1, bf16[256,2048]{1,0:T(8,128)(2,1)} %wo.1, ...), custom_call_target="tpu_custom_call" | custom-call | tf_op jit(solution)/shard_map/layer/pallas_call | solution.py:517
  83.4 1.7 %hand_over.1 = (bf16[64,2048]{1,0:T(8,128)(2,1)}, f32[4,512]{1,0:T(4,128)}) custom-call(bf16[64,2048]{1,0:T(8,128)(2,1)} %get-tuple-element.4.out_in, f32[4,512]{1,0:T(4,128)} %get-tuple-element.5.lw_in), custom_call_target="tpu_custom_call" | custom-call | tf_op jit(solution)/shard_map/hand_over/pallas_call | solution.py:561

commit v4 on v3

--- a/solution.py
+++ b/solution.py
@@ -40,10 +40,10 @@
 R_WR = R_WD + 2 * 2 * 7
 R_X = R_WR + 2 * 2 * 2 * 2 * 4
 R_H = R_X + 16
-R_M = R_H + 2 * SLOTS
-R_A = R_M + 2 * SLOTS
+R_M = R_H + 4 * SLOTS
+R_A = R_M + 4 * SLOTS
 R_END = R_A + 2 * (NTP - 1)
-N_SEND = 140
+N_SEND = 160
 
 
 def dot(a, b, dims=NN):
@@ -84,10 +84,9 @@
     z_peer = [(((z + d) % NZ) * NY + y, tp) for d in range(NZ)]
     ahead = ((sp + 1) % NSP, tp)
     behind = ((sp + NSP - 1) % NSP, tp)
-    relay_of_me = y_peer[NY - 3]
-    relay_to = ((z * NY + (y + 3) % NY + 4) % NSP, tp)
-    source = (sp + NSP - 4) % NSP
-    relay_from = ((source // NY) * NY + (source % NY + NY - 3) % NY, tp)
+    relay_of_me = (((z + y // 4) % NZ) * NY + (y + NY - 3) % NY, tp)
+    source_y = (y + 3) % NY
+    relay_source = (((z + NZ - source_y // 4) % NZ) * NY + source_y, tp)
     t_peer = [(sp, (tp + d) % NTP) for d in range(NTP)]
     x_right = (sp, (tp + 2) % NTP)
     x_left = (sp, (tp + NTP - 2) % NTP)
@@ -111,7 +110,7 @@
     lw_copy = pltpu.make_async_copy(lw_out, lw_h, lsem.at[10])
 
     barrier = pltpu.get_barrier_semaphore()
-    partners = y_peer[1:] + z_peer[1:] + t_peer[1:] + [ahead, behind, relay_to, relay_from]
+    partners = y_peer[1:] + z_peer[1:] + t_peer[1:] + [ahead, behind, relay_of_me, relay_source]
     for dev in partners:
         pl.semaphore_signal(barrier, inc=1, device_id=dev, device_id_type=MESH)
     pl.semaphore_wait(barrier, len(partners))
@@ -204,29 +203,35 @@
         arrived(part_of(4, 0), R_X + 11)
         arrived(part_of(4, 1), R_X + 12)
 
-    def up_part(k, p):
-        return kv.at[k, p, :, 0:AHEAD_ROWS]
-
-    def down_part(k, p):
-        return kv.at[k, p, :, AHEAD_ROWS:ROWS]
+    def up_part(k, p, w):
+        return kv.at[k, p, w, 0:AHEAD_ROWS]
+
+    def down_part(k, p, w):
+        return kv.at[k, p, w, AHEAD_ROWS:ROWS]
+
+    def halo_sem(base, p, k, w):
+        return base + (p * SLOTS + k) * 2 + w
 
     def halo_send(p):
-        start(up_part(0, p), up_part(1, p), R_H + p * SLOTS + 1, ahead)
-        start(down_part(0, p), passing.at[p], R_M + p * SLOTS, relay_of_me)
+        for w in range(2):
+            start(up_part(0, p, w), up_part(1, p, w), halo_sem(R_H, p, 1, w), ahead)
+            start(down_part(0, p, w), passing.at[p, w], halo_sem(R_M, p, 0, w), relay_of_me)
 
     def up(p, k):
-        arrived(up_part(k, p), R_H + p * SLOTS + k)
-        if k < SLOTS - 1:
-            start(up_part(k, p), up_part(k + 1, p), R_H + p * SLOTS + k + 1, ahead)
+        for w in range(2):
+            arrived(up_part(k, p, w), halo_sem(R_H, p, k, w))
+            if k < SLOTS - 1:
+                start(up_part(k, p, w), up_part(k + 1, p, w), halo_sem(R_H, p, k + 1, w), ahead)
 
     def down(p, k):
-        if k == 0:
-            arrived(passing.at[p], R_M + p * SLOTS)
-            start(passing.at[p], down_part(4, p), R_M + p * SLOTS + 4, relay_to)
-        else:
-            arrived(down_part(k, p), R_M + p * SLOTS + k)
-            if k > 1:
-                start(down_part(k, p), down_part(k - 1, p), R_M + p * SLOTS + k - 1, behind)
+        for w in range(2):
+            if k == 0:
+                arrived(passing.at[p, w], halo_sem(R_M, p, 0, w))
+                start(passing.at[p, w], down_part(4, p, w), halo_sem(R_M, p, 4, w), y_peer[NY - 1])
+            else:
+                arrived(down_part(k, p, w), halo_sem(R_M, p, k, w))
+                if k > 1:
+                    start(down_part(k, p, w), down_part(k - 1, p, w), halo_sem(R_M, p, k - 1, w), behind)
 
     lane = lax.broadcasted_iota(jnp.int32, (1, 128), 1)
     first_head = lane < 64
@@ -394,13 +399,12 @@
                 lw_s[rows, :] = jnp.where(lane < 2, lw_s[rows, :], both)
         att_n[p] = dot(perm[1], att_p[...]).astype(BF16)
         att_all[p, tp] = att_n[p, pl.ds(pl.multiple_of(tp * OUT_ROWS, OUT_ROWS), OUT_ROWS), :]
-        for d in range(1, NTP):
+        for d in (4, 3, 5, 2, 6, 1, 7):
             rows = pl.ds(pl.multiple_of(((tp + d) % NTP) * OUT_ROWS, OUT_ROWS), OUT_ROWS)
             start(att_n.at[p, rows], att_all.at[p, tp], R_A + p * (NTP - 1) + d - 1, t_peer[d])
 
-    def attended_wait(p):
-        for d in range(1, NTP):
-            arrived(att_all.at[p, (tp + NTP - d) % NTP], R_A + p * (NTP - 1) + d - 1)
+    def attended_wait(p, d):
+        arrived(att_all.at[p, (tp + NTP - d) % NTP], R_A + p * (NTP - 1) + d - 1)
 
     def log_weights():
         levels = jnp.transpose(lw_s[...])[0:8, :]
@@ -412,21 +416,22 @@
         lw_out[...] = natural[0:4, :]
         lw_copy.start()
 
-    def project():
-        def step(c, squares):
-            cols = pl.ds(pl.multiple_of(c * 512, 512), 512)
-            total = None
-            for g in range(NTP):
-                a = jnp.concatenate([att_all[0, g], att_all[1, g]], axis=1)
-                part = dot(a, wo_v[g, :, cols]).astype(BF16).astype(F32)
-                total = part if total is None else total + part
-            sum_s[:, cols] = total
-            return squares + jnp.sum(total * total, axis=-1, keepdims=True)
-
-        squares = lax.fori_loop(0, 4, step, jnp.zeros((OUT_ROWS, 1), F32))
-        scale = lax.rsqrt(squares / D + EPS)
+    def project(d):
+        if d:
+            attended_wait(0, d)
+            attended_wait(1, d)
+        g = (tp + NTP - d) % NTP
+        a = jnp.concatenate([att_all[0, g], att_all[1, g]], axis=1)
+        for c in range(2):
+            cols = slice(c * 1024, c * 1024 + 1024)
+            part = dot(a, wo_v[g, :, cols]).astype(BF16).astype(F32)
+            sum_s[:, cols] = part if d == 0 else sum_s[:, cols] + part
+
+    def output():
         local[9].wait()
-        out[...] = (sum_s[...] * scale * post[...]).astype(BF16)
+        total = sum_s[...]
+        scale = lax.rsqrt(jnp.mean(total * total, axis=-1, keepdims=True) + EPS)
+        out[...] = (total * scale * post[...]).astype(BF16)
         out_copy = pltpu.make_async_copy(out, out_h, lsem.at[11])
         out_copy.start()
         lw_copy.wait()
@@ -496,10 +501,16 @@
     near(1, 0, 1)
     finish(1)
     wo_sibling_wait()
-    attended_wait(0)
+    project(0)
     log_weights()
-    attended_wait(1)
-    project()
+    project(1)
+    project(7)
+    project(2)
+    project(6)
+    project(3)
+    project(5)
+    project(4)
+    output()
     for copy in sends:
         copy.wait_send()
 

time: 85.2 us -> 81.6 us (0.958)
  Pallas kernels: 84.4 us -> 80.8 us
    pallas_call x1, Pallas kernels: 82.7 us -> 79.1 us  [body(): pl.pallas_call(kernel, out_shape=(jax.ShapeDtypeStruct((OUT_ROWS, D), BF1...]
where the time goes in v4:
time: 81.6 us; the launch traced here: 81.5 us
  Pallas kernels  80.8 us (99%)
    pallas_call x1, Pallas kernels, body(): pl.pallas_call(kernel, out_shape=(jax.ShapeDtypeStruct((OUT_ROWS, D), BF1...  79.1 us
    pallas_call x1, Pallas kernels, body(): pl.pallas_call(hand_over, out_shape=(jax.ShapeDtypeStruct((OUT_ROWS, D),...  1.68 us

profile of v4, /device:TPU:1, one launch (start us, length us, event | category | flops | bytes accessed | tf_op | source)
XLA Modules:
  0.0 81.5 jit_solution(15023401200596067156)
XLA Ops:
  0.6 79.1 %layer.1 = (bf16[64,2048]{1,0:T(8,128)(2,1)}, f32[4,512]{1,0:T(4,128)}) custom-call(bf16[512,2048]{1,0:T(8,128)(2,1)} %hid.1, f32[1,2048]{1,0:T(1,128)} %bitcast.2, f32[1,128]{1,0:T(1,128)} %constant.2.clone.freq_h, bf16[2048,256]{1,0:T(8,128)(2,1)} %wq.1, bf16[32,256]{1,0:T(8,128)(2,1)} %wk.1, bf16[32,256]{1,0:T(8,128)(2,1)} %wv.1, bf16[256,2048]{1,0:T(8,128)(2,1)} %wo.1, ...), custom_call_target="tpu_custom_call" | custom-call | tf_op jit(solution)/shard_map/layer/pallas_call | solution.py:528
  79.8 1.7 %hand_over.1 = (bf16[64,2048]{1,0:T(8,128)(2,1)}, f32[4,512]{1,0:T(4,128)}) custom-call(bf16[64,2048]{1,0:T(8,128)(2,1)} %get-tuple-element.4.out_in, f32[4,512]{1,0:T(4,128)} %get-tuple-element.5.lw_in), custom_call_target="tpu_custom_call" | custom-call | tf_op jit(solution)/shard_map/hand_over/pallas_call | solution.py:572

commit v5 on v4

--- a/solution.py
+++ b/solution.py
@@ -37,13 +37,13 @@
 AHEAD_ROWS = 320
 
 R_WD = 0
-R_WR = R_WD + 2 * 2 * 7
-R_X = R_WR + 2 * 2 * 2 * 2 * 4
-R_H = R_X + 16
-R_M = R_H + 4 * SLOTS
+R_WR = R_WD + 4
+R_X = R_WR + 2 * 2 * 2 * 7
+R_H = R_X + 7
+R_M = R_H + 4 * (SLOTS - 1)
 R_A = R_M + 4 * SLOTS
-R_END = R_A + 2 * (NTP - 1)
-N_SEND = 160
+R_END = R_A + 1 + (NTP - 1)
+S_WD, S_WR, S_X, S_H, S_M, S_A = range(6)
 
 
 def dot(a, b, dims=NN):
@@ -64,21 +64,24 @@
     tp = lax.axis_index("tp")
     z, y = sp // NY, sp % NY
     x, core = tp // 2, tp % 2
-    sends = []
-
-    def start(src, dst, ridx, dev):
-        copy = pltpu.make_async_remote_copy(
-            src_ref=src, dst_ref=dst, send_sem=ssem.at[len(sends)], recv_sem=rsem.at[ridx],
+
+    def start(src, dst, ridx, dev, kind):
+        pltpu.make_async_remote_copy(
+            src_ref=src, dst_ref=dst, send_sem=ssem.at[kind], recv_sem=rsem.at[ridx],
             device_id=dev, device_id_type=MESH,
+        ).start()
+
+    def finished(size, ridx, kind):
+        return pltpu.make_async_remote_copy(
+            src_ref=size, dst_ref=size, send_sem=ssem.at[kind], recv_sem=rsem.at[ridx],
+            device_id=((sp + 1) % NSP, tp), device_id_type=MESH,
         )
-        copy.start()
-        sends.append(copy)
 
     def arrived(dst, ridx):
-        pltpu.make_async_remote_copy(
-            src_ref=dst, dst_ref=dst, send_sem=ssem.at[0], recv_sem=rsem.at[ridx],
-            device_id=((sp + 1) % NSP, tp), device_id_type=MESH,
-        ).wait_recv()
+        finished(dst, ridx, 0).wait_recv()
+
+    def sent(size, kind):
+        finished(size, 0, kind).wait_send()
 
     y_peer = [(z * NY + (y + d) % NY, tp) for d in range(NY)]
     z_peer = [(((z + d) % NZ) * NY + y, tp) for d in range(NZ)]
@@ -120,19 +123,18 @@
             local[2 * p + i].wait()
             part = w_v.at[i, p, z, y]
             for d in range(1, 8):
-                start(part, part, R_WD + (i * 2 + p) * 7 + d - 1, peer[d])
+                start(part, part, R_WD + i * 2 + p, peer[d], S_WD)
 
     def weights_wait(p):
-        for d in range(1, 8):
-            arrived(w_v.at[0, p, z, (y + NY - d) % NY], R_WD + p * 7 + d - 1)
-            arrived(w_v.at[1, p, (z + NZ - d) % NZ, y], R_WD + (2 + p) * 7 + d - 1)
+        for i in range(2):
+            arrived(w_v.at[i, p, 0, 0:7], R_WD + i * 2 + p)
 
     def relay_part(i, p, at, half):
         piece = pl.ds(half * 4, 4)
         return w_v.at[0, p, at, piece] if i == 0 else w_v.at[1, p, piece, at]
 
     def relay_sem(i, p, half, direction, hop):
-        return R_WR + (((i * 2 + p) * 2 + half) * 2 + direction) * 4 + hop
+        return R_WR + ((i * 2 + p) * 2 + half) * 7 + (hop if direction == 0 else 6 - hop)
 
     def relay_dev(i, direction):
         peer = z_peer if i == 0 else y_peer
@@ -143,7 +145,7 @@
             for i, at in enumerate((z, y)):
                 part = relay_part(i, p, at, half)
                 for direction in range(2):
-                    start(part, part, relay_sem(i, p, half, direction, 0), relay_dev(i, direction))
+                    start(part, part, relay_sem(i, p, half, direction, 0), relay_dev(i, direction), S_WR)
 
     def relay_step(p, hop):
         for half in range(2):
@@ -155,7 +157,7 @@
                         part = relay_part(i, p, owner, half)
                         arrived(part, relay_sem(i, p, half, direction, hop))
                         if hop + 1 < hops:
-                            start(part, part, relay_sem(i, p, half, direction, hop + 1), relay_dev(i, direction))
+                            start(part, part, relay_sem(i, p, half, direction, hop + 1), relay_dev(i, direction), S_WR)
 
     def wo_part(delta, part):
         group = wo_v.at[(tp + delta) % NTP]
@@ -163,45 +165,33 @@
 
     def wo_send():
         local[4].wait()
-        start(wo_part(0, 0), wo_part(0, 0), R_X + 0, x_right)
-        start(wo_part(0, 1), wo_part(0, 1), R_X + 1, x_left)
-        start(wo_part(0, 1), wo_part(0, 1), R_X + 2, x_right)
-        start(wo_part(0, 0), wo_part(0, 0), R_X + 3, x_left)
-        start(wo_part(0, None), wo_part(0, None), R_X + 6, sibling)
+        start(wo_part(0, 0), wo_part(0, 0), R_X + 0, x_right, S_X)
+        start(wo_part(0, 1), wo_part(0, 1), R_X + 1, x_left, S_X)
+        start(wo_part(0, 1), wo_part(0, 1), R_X + 2, x_right, S_X)
+        start(wo_part(0, 0), wo_part(0, 0), R_X + 3, x_left, S_X)
+        start(wo_part(0, None), wo_part(0, None), R_X + 6, sibling, S_X)
 
     def wo_step(k):
         if k == 0:
             arrived(wo_part(6, 0), R_X + 0)
-            start(wo_part(6, 0), wo_part(6, 0), R_X + 4, x_right)
-            start(wo_part(6, 0), wo_part(6, 0), R_X + 7, sibling)
+            start(wo_part(6, 0), wo_part(6, 0), R_X + 4, x_right, S_X)
+            start(wo_part(6, 0), wo_part(6, 0), R_X + 6, sibling, S_X)
             arrived(wo_part(2, 1), R_X + 1)
-            start(wo_part(2, 1), wo_part(2, 1), R_X + 5, x_left)
-            start(wo_part(2, 1), wo_part(2, 1), R_X + 8, sibling)
+            start(wo_part(2, 1), wo_part(2, 1), R_X + 5, x_left, S_X)
+            start(wo_part(2, 1), wo_part(2, 1), R_X + 6, sibling, S_X)
         elif k == 1:
             arrived(wo_part(6, 1), R_X + 2)
-            start(wo_part(6, 1), wo_part(6, 1), R_X + 9, sibling)
+            start(wo_part(6, 1), wo_part(6, 1), R_X + 6, sibling, S_X)
             arrived(wo_part(2, 0), R_X + 3)
-            start(wo_part(2, 0), wo_part(2, 0), R_X + 10, sibling)
+            start(wo_part(2, 0), wo_part(2, 0), R_X + 6, sibling, S_X)
         else:
             arrived(wo_part(4, 0), R_X + 4)
-            start(wo_part(4, 0), wo_part(4, 0), R_X + 11, sibling)
+            start(wo_part(4, 0), wo_part(4, 0), R_X + 6, sibling, S_X)
             arrived(wo_part(4, 1), R_X + 5)
-            start(wo_part(4, 1), wo_part(4, 1), R_X + 12, sibling)
+            start(wo_part(4, 1), wo_part(4, 1), R_X + 6, sibling, S_X)
 
     def wo_sibling_wait():
-        other = x * 2 + (1 - core)
-
-        def part_of(delta, part):
-            group = wo_v.at[(other + delta) % NTP]
-            return group if part is None else group.at[pl.ds(part * 128, 128)]
-
-        arrived(part_of(0, None), R_X + 6)
-        arrived(part_of(6, 0), R_X + 7)
-        arrived(part_of(2, 1), R_X + 8)
-        arrived(part_of(6, 1), R_X + 9)
-        arrived(part_of(2, 0), R_X + 10)
-        arrived(part_of(4, 0), R_X + 11)
-        arrived(part_of(4, 1), R_X + 12)
+        arrived(wo_v.at[0:4], R_X + 6)
 
     def up_part(k, p, w):
         return kv.at[k, p, w, 0:AHEAD_ROWS]
@@ -209,29 +199,32 @@
     def down_part(k, p, w):
         return kv.at[k, p, w, AHEAD_ROWS:ROWS]
 
-    def halo_sem(base, p, k, w):
-        return base + (p * SLOTS + k) * 2 + w
+    def up_sem(p, k, w):
+        return R_H + (p * (SLOTS - 1) + k - 1) * 2 + w
+
+    def down_sem(p, k, w):
+        return R_M + (p * SLOTS + k) * 2 + w
 
     def halo_send(p):
         for w in range(2):
-            start(up_part(0, p, w), up_part(1, p, w), halo_sem(R_H, p, 1, w), ahead)
-            start(down_part(0, p, w), passing.at[p, w], halo_sem(R_M, p, 0, w), relay_of_me)
+            start(up_part(0, p, w), up_part(1, p, w), up_sem(p, 1, w), ahead, S_H)
+            start(down_part(0, p, w), passing.at[p, w], down_sem(p, 0, w), relay_of_me, S_M)
 
     def up(p, k):
         for w in range(2):
-            arrived(up_part(k, p, w), halo_sem(R_H, p, k, w))
+            arrived(up_part(k, p, w), up_sem(p, k, w))
             if k < SLOTS - 1:
-                start(up_part(k, p, w), up_part(k + 1, p, w), halo_sem(R_H, p, k + 1, w), ahead)
+                start(up_part(k, p, w), up_part(k + 1, p, w), up_sem(p, k + 1, w), ahead, S_H)
 
     def down(p, k):
         for w in range(2):
             if k == 0:
-                arrived(passing.at[p, w], halo_sem(R_M, p, 0, w))
-                start(passing.at[p, w], down_part(4, p, w), halo_sem(R_M, p, 4, w), y_peer[NY - 1])
+                arrived(passing.at[p, w], down_sem(p, 0, w))
+                start(passing.at[p, w], down_part(4, p, w), down_sem(p, 4, w), y_peer[NY - 1], S_M)
             else:
-                arrived(down_part(k, p, w), halo_sem(R_M, p, k, w))
+                arrived(down_part(k, p, w), down_sem(p, k, w))
                 if k > 1:
-                    start(down_part(k, p, w), down_part(k - 1, p, w), halo_sem(R_M, p, k - 1, w), behind)
+                    start(down_part(k, p, w), down_part(k - 1, p, w), down_sem(p, k - 1, w), behind, S_M)
 
     lane = lax.broadcasted_iota(jnp.int32, (1, 128), 1)
     first_head = lane < 64
@@ -401,10 +394,7 @@
         att_all[p, tp] = att_n[p, pl.ds(pl.multiple_of(tp * OUT_ROWS, OUT_ROWS), OUT_ROWS), :]
         for d in (4, 3, 5, 2, 6, 1, 7):
             rows = pl.ds(pl.multiple_of(((tp + d) % NTP) * OUT_ROWS, OUT_ROWS), OUT_ROWS)
-            start(att_n.at[p, rows], att_all.at[p, tp], R_A + p * (NTP - 1) + d - 1, t_peer[d])
-
-    def attended_wait(p, d):
-        arrived(att_all.at[p, (tp + NTP - d) % NTP], R_A + p * (NTP - 1) + d - 1)
+            start(att_n.at[p, rows], att_all.at[p, tp], R_A + p * d, t_peer[d], S_A)
 
     def log_weights():
         levels = jnp.transpose(lw_s[...])[0:8, :]
@@ -417,10 +407,11 @@
         lw_copy.start()
 
     def project(d):
+        g = (tp + NTP - d) % NTP
+        if d == 1:
+            arrived(att_all.at[0, 0:7], R_A)
         if d:
-            attended_wait(0, d)
-            attended_wait(1, d)
-        g = (tp + NTP - d) % NTP
+            arrived(att_all.at[1, g], R_A + d)
         a = jnp.concatenate([att_all[0, g], att_all[1, g]], axis=1)
         for c in range(2):
             cols = slice(c * 1024, c * 1024 + 1024)
@@ -511,8 +502,12 @@
     project(5)
     project(4)
     output()
-    for copy in sends:
-        copy.wait_send()
+    sent(w_v.at[0, 0, 0:4, 0:7], S_WD)
+    sent(w_v.at[:, :, 0:7], S_WR)
+    sent(wo_v.at[0:7], S_X)
+    sent(kv.at[0:4, :, :, 0:AHEAD_ROWS], S_H)
+    sent(kv.at[:, :, :, AHEAD_ROWS:ROWS], S_M)
+    sent(att_all.at[:, 0:7], S_A)
 
 
 def hand_over(out_in, lw_in, out, lw_out):
@@ -558,7 +553,7 @@
             pltpu.VMEM((2, ROWS, ROWS), BF16),
             pltpu.VMEM((OUT_ROWS, D), F32),
             pltpu.SemaphoreType.DMA((12,)),
-            pltpu.SemaphoreType.DMA((N_SEND,)),
+            pltpu.SemaphoreType.DMA((6,)),
             pltpu.SemaphoreType.DMA((R_END,)),
         ],
         compiler_params=pltpu.CompilerParams(

time: 81.6 us -> 79.5 us (0.974)
  Pallas kernels: 80.8 us -> 78.7 us
    pallas_call x1, Pallas kernels: 79.1 us -> 77 us  [body(): pl.pallas_call(kernel, out_shape=(jax.ShapeDtypeStruct((OUT_ROWS, D), BF1...]
where the time goes in v5:
time: 79.5 us; the launch traced here: 79.3 us
  Pallas kernels  78.7 us (99%)
    pallas_call x1, Pallas kernels, body(): pl.pallas_call(kernel, out_shape=(jax.ShapeDtypeStruct((OUT_ROWS, D), BF1...  77 us
    pallas_call x1, Pallas kernels, body(): pl.pallas_call(hand_over, out_shape=(jax.ShapeDtypeStruct((OUT_ROWS, D),...  1.68 us

profile of v5, /device:TPU:1, one launch (start us, length us, event | category | flops | bytes accessed | tf_op | source)
XLA Modules:
  0.0 79.3 jit_solution(13159651415686545483)
XLA Ops:
  0.6 77.0 %layer.1 = (bf16[64,2048]{1,0:T(8,128)(2,1)}, f32[4,512]{1,0:T(4,128)}) custom-call(bf16[512,2048]{1,0:T(8,128)(2,1)} %hid.1, f32[1,2048]{1,0:T(1,128)} %bitcast.2, f32[1,128]{1,0:T(1,128)} %constant.2.clone.freq_h, bf16[2048,256]{1,0:T(8,128)(2,1)} %wq.1, bf16[32,256]{1,0:T(8,128)(2,1)} %wk.1, bf16[32,256]{1,0:T(8,128)(2,1)} %wv.1, bf16[256,2048]{1,0:T(8,128)(2,1)} %wo.1, ...), custom_call_target="tpu_custom_call" | custom-call | tf_op jit(solution)/shard_map/layer/pallas_call | solution.py:523
  77.7 1.7 %hand_over.1 = (bf16[64,2048]{1,0:T(8,128)(2,1)}, f32[4,512]{1,0:T(4,128)}) custom-call(bf16[64,2048]{1,0:T(8,128)(2,1)} %get-tuple-element.4.out_in, f32[4,512]{1,0:T(4,128)} %get-tuple-element.5.lw_in), custom_call_target="tpu_custom_call" | custom-call | tf_op jit(solution)/shard_map/hand_over/pallas_call | solution.py:567

commit v6 on v5

--- a/solution.py
+++ b/solution.py
@@ -122,7 +122,7 @@
         for i, peer in enumerate((y_peer, z_peer)):
             local[2 * p + i].wait()
             part = w_v.at[i, p, z, y]
-            for d in range(1, 8):
+            for d in (4, 3, 5, 2, 6, 1, 7):
                 start(part, part, R_WD + i * 2 + p, peer[d], S_WD)
 
     def weights_wait(p):
@@ -140,24 +140,25 @@
         peer = z_peer if i == 0 else y_peer
         return peer[1] if direction == 0 else peer[7]
 
-    def relay_send(p):
-        for half in range(2):
-            for i, at in enumerate((z, y)):
-                part = relay_part(i, p, at, half)
-                for direction in range(2):
-                    start(part, part, relay_sem(i, p, half, direction, 0), relay_dev(i, direction), S_WR)
-
-    def relay_step(p, hop):
-        for half in range(2):
+    def relay_order():
+        for late in range(2):
             for i, at in enumerate((z, y)):
                 for direction in range(2):
-                    hops = 4 if half == direction else 3
-                    if hop < hops:
-                        owner = (at + 7 - hop) % 8 if direction == 0 else (at + 1 + hop) % 8
-                        part = relay_part(i, p, owner, half)
-                        arrived(part, relay_sem(i, p, half, direction, hop))
-                        if hop + 1 < hops:
-                            start(part, part, relay_sem(i, p, half, direction, hop + 1), relay_dev(i, direction), S_WR)
+                    yield direction ^ late, i, at, direction, 4 - late
+
+    def relay_send(p):
+        for half, i, at, direction, _ in relay_order():
+            part = relay_part(i, p, at, half)
+            start(part, part, relay_sem(i, p, half, direction, 0), relay_dev(i, direction), S_WR)
+
+    def relay_step(p, hop):
+        for half, i, at, direction, hops in relay_order():
+            if hop < hops:
+                owner = (at + 7 - hop) % 8 if direction == 0 else (at + 1 + hop) % 8
+                part = relay_part(i, p, owner, half)
+                arrived(part, relay_sem(i, p, half, direction, hop))
+                if hop + 1 < hops:
+                    start(part, part, relay_sem(i, p, half, direction, hop + 1), relay_dev(i, direction), S_WR)
 
     def wo_part(delta, part):
         group = wo_v.at[(tp + delta) % NTP]
@@ -205,16 +206,34 @@
     def down_sem(p, k, w):
         return R_M + (p * SLOTS + k) * 2 + w
 
+    def clear():
+        for k in range(1, SLOTS):
+
+            @pl.when(sp < k)
+            def _():
+                kv[k, :, :, 0:AHEAD_ROWS] = jnp.zeros((2, 2, AHEAD_ROWS, 128), BF16)
+
     def halo_send(p):
+        @pl.when(sp < NSP - 1)
+        def _():
+            for w in range(2):
+                start(up_part(0, p, w), up_part(1, p, w), up_sem(p, 1, w), ahead, S_H)
+
         for w in range(2):
-            start(up_part(0, p, w), up_part(1, p, w), up_sem(p, 1, w), ahead, S_H)
             start(down_part(0, p, w), passing.at[p, w], down_sem(p, 0, w), relay_of_me, S_M)
 
     def up(p, k):
         for w in range(2):
-            arrived(up_part(k, p, w), up_sem(p, k, w))
+
+            @pl.when(sp >= k)
+            def _():
+                arrived(up_part(k, p, w), up_sem(p, k, w))
+
             if k < SLOTS - 1:
-                start(up_part(k, p, w), up_part(k + 1, p, w), up_sem(p, k + 1, w), ahead, S_H)
+
+                @pl.when((sp >= k) & (sp < NSP - 1))
+                def _():
+                    start(up_part(k, p, w), up_part(k + 1, p, w), up_sem(p, k + 1, w), ahead, S_H)
 
     def down(p, k):
         for w in range(2):
@@ -379,17 +398,18 @@
 
         lax.fori_loop(first, last, step, 0, unroll=True)
 
+    def levels(p):
+        for r in range(4):
+            rows = slice(r * 128, (r + 1) * 128)
+            level = st_m[p, r] * LN2 + jnp.log(st_l[p, r])
+            both = jnp.where(lane == 2 * p, level[0:128], level[128:256])
+            lw_s[rows, :] = both if p == 0 else jnp.where(lane < 2, lw_s[rows, :], both)
+
     def finish(p):
         for r in range(4):
             rows = slice(r * 128, (r + 1) * 128)
             o = st_o[p, r] / st_l[p, r]
             att_p[rows, :] = jnp.where(first_head, o[0:128], o[128:256]).astype(BF16)
-            level = st_m[p, r] * LN2 + jnp.log(st_l[p, r])
-            both = jnp.where(lane == 2 * p, level[0:128], level[128:256])
-            if p == 0:
-                lw_s[rows, :] = both
-            else:
-                lw_s[rows, :] = jnp.where(lane < 2, lw_s[rows, :], both)
         att_n[p] = dot(perm[1], att_p[...]).astype(BF16)
         att_all[p, tp] = att_n[p, pl.ds(pl.multiple_of(tp * OUT_ROWS, OUT_ROWS), OUT_ROWS), :]
         for d in (4, 3, 5, 2, 6, 1, 7):
@@ -433,6 +453,7 @@
     wo_send()
     norm()
     permutation()
+    clear()
     permute()
     weights_wait(0)
     relay_send(0)
@@ -477,14 +498,14 @@
     up(1, 3)
     far(1, 3, 4, (3, 4))
     down(0, 2)
+    down(1, 2)
     up(0, 4)
-    far(0, 0, 2, (3, 4))
-    down(1, 2)
-    far(0, 2, 3, (3, 4))
+    far(0, 0, 3, (3, 4))
     down(0, 1)
     far(0, 2, 4, (1, 2))
     near(0, 0, 1)
     finish(0)
+    levels(0)
     up(1, 4)
     far(1, 0, 3, (3, 4))
     down(1, 1)
@@ -493,6 +514,7 @@
     finish(1)
     wo_sibling_wait()
     project(0)
+    levels(1)
     log_weights()
     project(1)
     project(7)
@@ -505,7 +527,12 @@
     sent(w_v.at[0, 0, 0:4, 0:7], S_WD)
     sent(w_v.at[:, :, 0:7], S_WR)
     sent(wo_v.at[0:7], S_X)
-    sent(kv.at[0:4, :, :, 0:AHEAD_ROWS], S_H)
+    for k in range(SLOTS - 1):
+
+        @pl.when((sp >= k) & (sp < NSP - 1))
+        def _():
+            sent(kv.at[k, :, :, 0:AHEAD_ROWS], S_H)
+
     sent(kv.at[:, :, :, AHEAD_ROWS:ROWS], S_M)
     sent(att_all.at[:, 0:7], S_A)
 

time: 79.5 us -> 76 us (0.956)
  Pallas kernels: 78.7 us -> 75.1 us
    pallas_call x1, Pallas kernels: 77 us -> 73.4 us  [body(): pl.pallas_call(kernel, out_shape=(jax.ShapeDtypeStruct((OUT_ROWS, D), BF1...]
where the time goes in v6:
time: 76 us; the launch traced here: 75.8 us
  Pallas kernels  75.1 us (99%)
    pallas_call x1, Pallas kernels, body(): pl.pallas_call(kernel, out_shape=(jax.ShapeDtypeStruct((OUT_ROWS, D), BF1...  73.4 us
    pallas_call x1, Pallas kernels, body(): pl.pallas_call(hand_over, out_shape=(jax.ShapeDtypeStruct((OUT_ROWS, D),...  1.68 us

profile of v6, /device:TPU:1, one launch (start us, length us, event | category | flops | bytes accessed | tf_op | source)
XLA Modules:
  0.0 75.8 jit_solution(10829140601093465624)
XLA Ops:
  0.6 73.4 %layer.1 = (bf16[64,2048]{1,0:T(8,128)(2,1)}, f32[4,512]{1,0:T(4,128)}) custom-call(bf16[512,2048]{1,0:T(8,128)(2,1)} %hid.1, f32[1,2048]{1,0:T(1,128)} %bitcast.2, f32[1,128]{1,0:T(1,128)} %constant.2.clone.freq_h, bf16[2048,256]{1,0:T(8,128)(2,1)} %wq.1, bf16[32,256]{1,0:T(8,128)(2,1)} %wk.1, bf16[32,256]{1,0:T(8,128)(2,1)} %wv.1, bf16[256,2048]{1,0:T(8,128)(2,1)} %wo.1, ...), custom_call_target="tpu_custom_call" | custom-call | tf_op jit(solution)/shard_map/layer/pallas_call | solution.py:550
  74.1 1.7 %hand_over.1 = (bf16[64,2048]{1,0:T(8,128)(2,1)}, f32[4,512]{1,0:T(4,128)}) custom-call(bf16[64,2048]{1,0:T(8,128)(2,1)} %get-tuple-element.4.out_in, f32[4,512]{1,0:T(4,128)} %get-tuple-element.5.lw_in), custom_call_target="tpu_custom_call" | custom-call | tf_op jit(solution)/shard_map/hand_over/pallas_call | solution.py:594

commit v7 on v6

--- a/solution.py
+++ b/solution.py
@@ -56,8 +56,8 @@
 
 def kernel(
     hid, gain_h, freq_h, wq, wk, wv, wo, post_h,
-    out_h, lw_h,
-    gain, freq, post, out, lw_out, hid_v, np_v, wq_v, w_v, wo_v, kv, passing, q_s, st_o, st_m, st_l, att_p, att_n, att_all, lw_s,
+    out, lw_out,
+    gain, freq, post, hid_v, np_v, wq_v, w_v, wo_v, kv, passing, q_s, st_o, st_m, st_l, att_p, att_n, att_all, lw_s,
     cos_s, sin_s, bias_c, bias_n, perm, sum_s, lsem, ssem, rsem,
 ):
     sp = lax.axis_index("sp")
@@ -109,8 +109,6 @@
     ]
     for copy in local:
         copy.start()
-
-    lw_copy = pltpu.make_async_copy(lw_out, lw_h, lsem.at[10])
 
     barrier = pltpu.get_barrier_semaphore()
     partners = y_peer[1:] + z_peer[1:] + t_peer[1:] + [ahead, behind, relay_of_me, relay_source]
@@ -424,7 +422,6 @@
         low = (rest - mid.astype(F32)).astype(BF16)
         natural = dot(high, perm[0]) + dot(mid, perm[0]) + dot(low, perm[0])
         lw_out[...] = natural[0:4, :]
-        lw_copy.start()
 
     def project(d):
         g = (tp + NTP - d) % NTP
@@ -443,10 +440,6 @@
         total = sum_s[...]
         scale = lax.rsqrt(jnp.mean(total * total, axis=-1, keepdims=True) + EPS)
         out[...] = (total * scale * post[...]).astype(BF16)
-        out_copy = pltpu.make_async_copy(out, out_h, lsem.at[11])
-        out_copy.start()
-        lw_copy.wait()
-        out_copy.wait()
 
     weights_send(0)
     weights_send(1)
@@ -545,19 +538,17 @@
 def body(hidden_in, pre_gain, query_proj, key_proj, value_proj, out_proj, post_gain):
     half = np.arange(HEAD_DIM // 2, dtype=np.float32) * np.float32(2.0) / np.float32(HEAD_DIM)
     freq = np.tile(np.power(np.float64(ROPE_BASE), -half.astype(np.float64)).astype(np.float32), 4).reshape(1, 128)
-    any_spec = pl.BlockSpec(memory_space=pl.ANY)
+    hbm = pl.BlockSpec(memory_space=pltpu.HBM)
     vmem = pl.BlockSpec(memory_space=pltpu.VMEM)
     results = pl.pallas_call(
         kernel,
         out_shape=(jax.ShapeDtypeStruct((OUT_ROWS, D), BF16), jax.ShapeDtypeStruct((4, ROWS), F32)),
-        in_specs=[any_spec] * 8,
-        out_specs=(any_spec, any_spec),
+        in_specs=[hbm] * 8,
+        out_specs=(vmem, vmem),
         scratch_shapes=[
             pltpu.VMEM((1, D), F32),
             pltpu.VMEM((1, 128), F32),
             pltpu.VMEM((1, D), F32),
-            pltpu.VMEM((OUT_ROWS, D), BF16),
-            pltpu.VMEM((4, ROWS), F32),
             pltpu.VMEM((ROWS, D), BF16),
             pltpu.VMEM((ROWS, D), BF16),
             pltpu.VMEM((D, WIDTH), BF16),
@@ -579,23 +570,27 @@
             pltpu.VMEM((2, 128, 256), F32),
             pltpu.VMEM((2, ROWS, ROWS), BF16),
             pltpu.VMEM((OUT_ROWS, D), F32),
-            pltpu.SemaphoreType.DMA((12,)),
+            pltpu.SemaphoreType.DMA((10,)),
             pltpu.SemaphoreType.DMA((6,)),
             pltpu.SemaphoreType.DMA((R_END,)),
         ],
         compiler_params=pltpu.CompilerParams(
-            collective_id=0, has_side_effects=True, vmem_limit_bytes=60 * 1024 * 1024
+            collective_id=0, has_side_effects=True, vmem_limit_bytes=53 * 1024 * 1024
         ),
         name="layer",
-    )(
-        hidden_in, pre_gain.reshape(1, D), jnp.asarray(freq), query_proj, key_proj, value_proj, out_proj,
-        post_gain.reshape(1, D),
-    )
+    )(*(
+        pltpu.with_memory_space_constraint(a, pltpu.HBM)
+        for a in (
+            hidden_in, pre_gain.reshape(1, D), jnp.asarray(freq), query_proj, key_proj, value_proj, out_proj,
+            post_gain.reshape(1, D),
+        )
+    ))
     return pl.pallas_call(
         hand_over,
         out_shape=(jax.ShapeDtypeStruct((OUT_ROWS, D), BF16), jax.ShapeDtypeStruct((4, ROWS), F32)),
         in_specs=[vmem, vmem],
         out_specs=(vmem, vmem),
+        compiler_params=pltpu.CompilerParams(vmem_limit_bytes=4 * 1024 * 1024),
         name="hand_over",
     )(*results)
 

time: 76 us -> 74.3 us (0.978)
  Pallas kernels: 75.1 us -> 73.5 us
    pallas_call x1, Pallas kernels: 1.68 us -> 0.72 us  [body(): pl.pallas_call(hand_over, out_shape=(jax.ShapeDtypeStruct((OUT_ROWS, D),...]
where the time goes in v7:
time: 74.3 us; the launch traced here: 74.1 us
  Pallas kernels  73.5 us (99%)
    pallas_call x1, Pallas kernels, body(): pl.pallas_call(kernel, out_shape=(jax.ShapeDtypeStruct((OUT_ROWS, D), BF1...  72.7 us

profile of v7, /device:TPU:1, one launch (start us, length us, event | category | flops | bytes accessed | tf_op | source)
XLA Modules:
  0.0 74.1 jit_solution(17968626778411309871)
XLA Ops:
  0.6 72.7 %layer.1 = (bf16[64,2048]{1,0:T(8,128)(2,1)S(1)}, f32[4,512]{1,0:T(4,128)S(1)}) custom-call(bf16[512,2048]{1,0:T(8,128)(2,1)} %hid.1, f32[1,2048]{1,0:T(1,128)} %bitcast.2, f32[1,128]{1,0:T(1,128)} %constant.2.clone.freq_h, bf16[2048,256]{1,0:T(8,128)(2,1)} %wq.1, bf16[32,256]{1,0:T(8,128)(2,1)} %wk.1, bf16[32,256]{1,0:T(8,128)(2,1)} %wv.1, ...), custom_call_target="tpu_custom_call" | custom-call | tf_op jit(solution)/shard_map/layer/pallas_call | solution.py:543
  73.4 0.7 hand_over.1

commit v8 on v7

--- a/solution.py
+++ b/solution.py
@@ -211,14 +211,20 @@
             def _():
                 kv[k, :, :, 0:AHEAD_ROWS] = jnp.zeros((2, 2, AHEAD_ROWS, 128), BF16)
 
+            @pl.when(sp == k - 1)
+            def _():
+                kv[k, :, :, AHEAD_ROWS:ROWS] = jnp.zeros((2, 2, ROWS - AHEAD_ROWS, 128), BF16)
+
     def halo_send(p):
         @pl.when(sp < NSP - 1)
         def _():
             for w in range(2):
                 start(up_part(0, p, w), up_part(1, p, w), up_sem(p, 1, w), ahead, S_H)
 
-        for w in range(2):
-            start(down_part(0, p, w), passing.at[p, w], down_sem(p, 0, w), relay_of_me, S_M)
+        @pl.when(sp != NSP - 1)
+        def _():
+            for w in range(2):
+                start(down_part(0, p, w), passing.at[p, w], down_sem(p, 0, w), relay_of_me, S_M)
 
     def up(p, k):
         for w in range(2):
@@ -234,14 +240,16 @@
                     start(up_part(k, p, w), up_part(k + 1, p, w), up_sem(p, k + 1, w), ahead, S_H)
 
     def down(p, k):
-        for w in range(2):
-            if k == 0:
-                arrived(passing.at[p, w], down_sem(p, 0, w))
-                start(passing.at[p, w], down_part(4, p, w), down_sem(p, 4, w), y_peer[NY - 1], S_M)
-            else:
-                arrived(down_part(k, p, w), down_sem(p, k, w))
-                if k > 1:
-                    start(down_part(k, p, w), down_part(k - 1, p, w), down_sem(p, k - 1, w), behind, S_M)
+        @pl.when(sp != (4 if k == 0 else k - 1))
+        def _():
+            for w in range(2):
+                if k == 0:
+                    arrived(passing.at[p, w], down_sem(p, 0, w))
+                    start(passing.at[p, w], down_part(4, p, w), down_sem(p, 4, w), y_peer[NY - 1], S_M)
+                else:
+                    arrived(down_part(k, p, w), down_sem(p, k, w))
+                    if k > 1:
+                        start(down_part(k, p, w), down_part(k - 1, p, w), down_sem(p, k - 1, w), behind, S_M)
 
     lane = lax.broadcasted_iota(jnp.int32, (1, 128), 1)
     first_head = lane < 64
@@ -526,7 +534,16 @@
         def _():
             sent(kv.at[k, :, :, 0:AHEAD_ROWS], S_H)
 
-    sent(kv.at[:, :, :, AHEAD_ROWS:ROWS], S_M)
+    one_short = (sp == NSP - 1) | ((sp >= 1) & (sp <= 4))
+
+    @pl.when(one_short)
+    def _():
+        sent(kv.at[0:4, :, :, AHEAD_ROWS:ROWS], S_M)
+
+    @pl.when(jnp.logical_not(one_short))
+    def _():
+        sent(kv.at[:, :, :, AHEAD_ROWS:ROWS], S_M)
+
     sent(att_all.at[:, 0:7], S_A)
 
 

time: 74.3 us -> 73 us (0.983)
  Pallas kernels: 73.5 us -> 71.8 us
    pallas_call x1, Pallas kernels: 72.7 us -> 71.1 us  [body(): pl.pallas_call(kernel, out_shape=(jax.ShapeDtypeStruct((OUT_ROWS, D), BF1...]
where the time goes in v8:
time: 73 us; the launch traced here: 72.5 us
  Pallas kernels  71.8 us (98%)
    pallas_call x1, Pallas kernels, body(): pl.pallas_call(kernel, out_shape=(jax.ShapeDtypeStruct((OUT_ROWS, D), BF1...  71.1 us

profile of v8, /device:TPU:1, one launch (start us, length us, event | category | flops | bytes accessed | tf_op | source)
XLA Modules:
  0.0 72.5 jit_solution(11813538516816310399)
XLA Ops:
  0.6 71.1 %layer.1 = (bf16[64,2048]{1,0:T(8,128)(2,1)S(1)}, f32[4,512]{1,0:T(4,128)S(1)}) custom-call(bf16[512,2048]{1,0:T(8,128)(2,1)} %hid.1, f32[1,2048]{1,0:T(1,128)} %bitcast.2, f32[1,128]{1,0:T(1,128)} %constant.2.clone.freq_h, bf16[2048,256]{1,0:T(8,128)(2,1)} %wq.1, bf16[32,256]{1,0:T(8,128)(2,1)} %wk.1, bf16[32,256]{1,0:T(8,128)(2,1)} %wv.1, ...), custom_call_target="tpu_custom_call" | custom-call | tf_op jit(solution)/shard_map/layer/pallas_call | solution.py:560
  71.7 0.7 hand_over.1

commit v9 on v8

--- a/solution.py
+++ b/solution.py
@@ -107,13 +107,12 @@
         pltpu.make_async_copy(freq_h, freq, lsem.at[8]),
         pltpu.make_async_copy(post_h, post, lsem.at[9]),
     ]
-    for copy in local:
-        copy.start()
-
     barrier = pltpu.get_barrier_semaphore()
     partners = y_peer[1:] + z_peer[1:] + t_peer[1:] + [ahead, behind, relay_of_me, relay_source]
     for dev in partners:
         pl.semaphore_signal(barrier, inc=1, device_id=dev, device_id_type=MESH)
+    for copy in local:
+        copy.start()
     pl.semaphore_wait(barrier, len(partners))
 
     def weights_send(p):
@@ -215,12 +214,13 @@
             def _():
                 kv[k, :, :, AHEAD_ROWS:ROWS] = jnp.zeros((2, 2, ROWS - AHEAD_ROWS, 128), BF16)
 
-    def halo_send(p):
+    def up_send(p):
         @pl.when(sp < NSP - 1)
         def _():
             for w in range(2):
                 start(up_part(0, p, w), up_part(1, p, w), up_sem(p, 1, w), ahead, S_H)
 
+    def down_send(p):
         @pl.when(sp != NSP - 1)
         def _():
             for w in range(2):
@@ -336,11 +336,10 @@
                     q_s[p, r0 // 128 + r, 0:128, :] = jnp.where(first_head, turned, zero)
                     q_s[p, r0 // 128 + r, 128:256, :] = jnp.where(first_head, zero, turned)
 
-    def keys_values(p):
+    def keys_values(p, first, last):
         weights = jnp.concatenate([w_v[i, p].reshape(D, 128) for i in range(2)], axis=1)
 
-        for r0 in range(0, ROWS, BIG):
-            rows = slice(r0, r0 + BIG)
+        for rows in (slice(first, last),):
             both = dot(np_v[rows, :], weights)
             kv[0, p, 0, rows, :] = rotate(both[:, 0:128], rows)
             kv[0, p, 1, rows, :] = both[:, 128:256].astype(BF16)
@@ -470,11 +469,14 @@
     relay_step(1, 2)
     wo_step(0)
     relay_step(0, 3)
-    keys_values(0)
-    halo_send(0)
+    keys_values(0, 0, AHEAD_ROWS)
+    up_send(0)
+    keys_values(0, AHEAD_ROWS, ROWS)
+    down_send(0)
     relay_step(1, 3)
-    keys_values(1)
-    halo_send(1)
+    keys_values(1, 0, ROWS)
+    up_send(1)
+    down_send(1)
     queries()
     far(0, 0, 4, (0,))
     near(0, 1, 4)

time: 73 us -> 72.7 us (level)
  no operation moved by 1% of the time
where the time goes in v9:
time: 72.7 us; the launch traced here: 72.6 us
  Pallas kernels  71.9 us (99%)
    pallas_call x1, Pallas kernels, body(): pl.pallas_call(kernel, out_shape=(jax.ShapeDtypeStruct((OUT_ROWS, D), BF1...  71.2 us

profile of v9, /device:TPU:1, one launch (start us, length us, event | category | flops | bytes accessed | tf_op | source)
XLA Modules:
  0.0 72.6 jit_solution(1022288473777597757)
XLA Ops:
  0.6 71.2 %layer.1 = (bf16[64,2048]{1,0:T(8,128)(2,1)S(1)}, f32[4,512]{1,0:T(4,128)S(1)}) custom-call(bf16[512,2048]{1,0:T(8,128)(2,1)} %hid.1, f32[1,2048]{1,0:T(1,128)} %bitcast.2, f32[1,128]{1,0:T(1,128)} %constant.2.clone.freq_h, bf16[2048,256]{1,0:T(8,128)(2,1)} %wq.1, bf16[32,256]{1,0:T(8,128)(2,1)} %wk.1, bf16[32,256]{1,0:T(8,128)(2,1)} %wv.1, ...), custom_call_target="tpu_custom_call" | custom-call | tf_op jit(solution)/shard_map/layer/pallas_call | solution.py:562
  71.9 0.7 hand_over.1

commit v10 on v9

--- a/solution.py
+++ b/solution.py
@@ -490,17 +490,17 @@
     up(0, 2)
     far(0, 0, 2, (1, 2))
     down(0, 4)
+    down(1, 4)
     up(1, 2)
     far(1, 0, 2, (1, 2))
-    down(1, 4)
     down(0, 3)
+    down(1, 3)
     up(0, 3)
     wo_step(2)
-    down(1, 3)
     far(0, 3, 4, (3, 4))
-    up(1, 3)
     far(1, 3, 4, (3, 4))
     down(0, 2)
+    up(1, 3)
     down(1, 2)
     up(0, 4)
     far(0, 0, 3, (3, 4))

time: 72.7 us -> 73.4 us (level)
  no operation moved by 1% of the time
where the time goes in v10:
time: 73.4 us; the launch traced here: 72.6 us
  Pallas kernels  71.9 us (98%)
    pallas_call x1, Pallas kernels, body(): pl.pallas_call(kernel, out_shape=(jax.ShapeDtypeStruct((OUT_ROWS, D), BF1...  71.2 us

profile of v10, /device:TPU:1, one launch (start us, length us, event | category | flops | bytes accessed | tf_op | source)
XLA Modules:
  0.0 72.6 jit_solution(3141933359124000640)
XLA Ops:
  0.6 71.2 %layer.1 = (bf16[64,2048]{1,0:T(8,128)(2,1)S(1)}, f32[4,512]{1,0:T(4,128)S(1)}) custom-call(bf16[512,2048]{1,0:T(8,128)(2,1)} %hid.1, f32[1,2048]{1,0:T(1,128)} %bitcast.2, f32[1,128]{1,0:T(1,128)} %constant.2.clone.freq_h, bf16[2048,256]{1,0:T(8,128)(2,1)} %wq.1, bf16[32,256]{1,0:T(8,128)(2,1)} %wk.1, bf16[32,256]{1,0:T(8,128)(2,1)} %wv.1, ...), custom_call_target="tpu_custom_call" | custom-call | tf_op jit(solution)/shard_map/layer/pallas_call | solution.py:562
  71.9 0.7 hand_over.1
